TPU v7x, 512 devices: a 8x2x16 block of a 8x8x16 slice. The times are simulated.
512 devices in a mesh: grp: 2 (over y), row: 32 (over z, core), col: 8 (over x).
Axes of the slice: x: 8, y: 2, z: 16, core: 2. Of those that a mesh axis runs over, the one named last changes fastest.
The devices are a block of a 8x8x16 slice.
Arguments:
- gate_one: bfloat16 [16384, 2048], P(('grp', 'row'), 'col'), parts along dimension 0, may hold values from -6 to 6
- gate_two: bfloat16 [16384, 2048], P(('grp', 'row'), 'col'), parts along dimension 0, may hold values from -6 to 6
- values: bfloat16 [16384, 2048], P(('grp', 'row'), 'col'), parts along dimension 0, may hold values from -6 to 6
- conv_taps: bfloat16 [3, 3, 2048], P(None, None, 'col'), may hold values from -3 to 3
- embed_weight: float32 [33, 128], replicated, may hold values from -12 to 12
- embed_bias: float32 [128], replicated, may hold values from -3.140625 to 3.140625
- sine_freq: float32 [128], replicated, may hold values from 0.1 to 1.9
- inner_weight: float32 [128, 128], replicated, may hold values from -6 to 6
- inner_bias: float32 [128], replicated, may hold values from -3.140625 to 3.140625
- filter_weight: float32 [128, 2, 2, 2048], P(None, None, None, 'col'), may hold values from -0.5 to 0.5
- decay_rate: float32 [2, 2, 2048], P(None, None, 'col'), may hold values from 0.3 to 655.36
- skip_gain: float32 [2, 2048], P(None, 'col'), may hold values from -4 to 4
- out_weight: bfloat16 [2048, 4096], P(None, 'col'), may hold values from -0.125 to 0.125
Outputs:
- mixed: bfloat16 [16384, 4096], P(('grp', 'row'), 'col'), parts along dimension 0
There are 2 independent parts, one for each index of `grp`. A program takes and returns all parts, laid end to end along the dimension named above; an argument that names none is the same for every part. Nothing has to cross between parts.
All inputs are finite; a program needn't handle non-finite values.
Results may differ from a plain program's by a relative error of at most 0.015.
Values may be sent and summed in bfloat16 or wider, within the bound.
No kernel may reach another device: no remote copies, remote signals or barrier semaphores. Data moves between devices by JAX's collectives and lax.ppermute only.
A program may use at most 64 MiB of HBM per device.

v0:
```python
import functools
import math

import jax
import jax.numpy as jnp
import numpy as np
from jax import lax
from jax.experimental import pallas as pl
from jax.experimental.pallas import tpu as pltpu
from jax.sharding import PartitionSpec as P

ENERGY_FLOOR = 1.0
F32 = jnp.float32
BF16 = jnp.bfloat16


def halves(value):
    high = value.astype(BF16)
    return high, (value - high.astype(F32)).astype(BF16)


def thirds(value):
    high = value.astype(BF16)
    rest = value - high.astype(F32)
    middle = rest.astype(BF16)
    return high, middle, (rest - middle.astype(F32)).astype(BF16)


def dot(left, right):
    return jnp.dot(left, right, preferred_element_type=F32)


def dot_three(left_high, left_low, right_high, right_low):
    return dot(left_high, right_high) + dot(left_low, right_high) + dot(left_high, right_low)


def cos_turns(turns):
    near = turns - jnp.round(turns)
    quarter = jnp.abs(near) - 0.25
    square = quarter * quarter
    total = jnp.full_like(square, SINE[-1])
    for factor in SINE[-2::-1]:
        total = total * square + factor
    return total * quarter


def fit_sine():
    nodes = 0.25 * np.cos(np.pi * (np.arange(64) + 0.5) / 128)
    powers = np.stack([nodes ** (2 * i + 1) for i in range(6)], 1)
    return [float(v) for v in np.linalg.lstsq(powers, -np.sin(2 * np.pi * nodes), rcond=None)[0]]


SINE = fit_sine()


def split_constant(table):
    high = table.astype(np.float32).astype(jnp.bfloat16)
    return np.stack([high, (table - high.astype(np.float64)).astype(np.float32).astype(jnp.bfloat16)])


@functools.lru_cache
def tables(rows, chan, block):
    waves = 2 * rows
    half = np.arange(rows + 1)
    phase = 2 * np.pi * (half[:, None] * np.arange(rows)[None] % waves) / waves
    weight = np.where((half == 0) | (half == rows), 1.0, 2.0)[:, None] / (waves * block)
    eye = np.eye(chan)
    into = np.concatenate([np.kron(np.cos(phase), eye), np.kron(-np.sin(phase[1:-1]), eye)])
    back = np.concatenate(
        [np.kron(weight * np.cos(phase), eye), np.kron(-(weight * np.sin(phase))[1:-1], eye)]
    ).T
    inner = 2 * np.pi * (np.arange(block)[:, None] * np.arange(block)[None] % block) / block
    fourier = np.concatenate([np.cos(inner), np.sin(inner)], 1)
    turn = 2 * np.pi * half[:, None] * np.arange(block)[None] / (waves * block)
    twiddle = np.stack([np.cos(turn), np.sin(turn)]).astype(np.float32)
    return split_constant(into), split_constant(back), split_constant(fourier), twiddle


def spread(twiddle_ref, part, chan):
    value = twiddle_ref[part]
    return jnp.broadcast_to(value[:, None, :], (value.shape[0], chan, value.shape[1])).reshape(-1, value.shape[1])


def forward(field, into_ref, fourier_ref, twiddle_ref, chan):
    block = field.shape[1]
    edge = field.shape[0] + chan
    high, low = halves(field)
    mixed = dot_three(into_ref[0], into_ref[1], high, low)
    zero = jnp.zeros((chan, block), F32)
    part_re = mixed[:edge]
    part_im = jnp.concatenate([zero, mixed[edge:], zero], 0)
    cos_part, sin_part = spread(twiddle_ref, 0, chan), spread(twiddle_ref, 1, chan)
    turned = jnp.concatenate(
        [part_re * cos_part + part_im * sin_part, part_im * cos_part - part_re * sin_part], 0
    )
    high, low = halves(turned)
    wave = dot_three(high, low, fourier_ref[0], fourier_ref[1])
    return wave[:edge, :block] + wave[edge:, block:], wave[edge:, :block] - wave[:edge, block:]


def backward(part_re, part_im, back_ref, fourier_ref, twiddle_ref, chan):
    edge, block = part_re.shape
    high, low = halves(jnp.concatenate([part_re, part_im], 0))
    wave = dot_three(high, low, fourier_ref[0], fourier_ref[1])
    part_re = wave[:edge, :block] - wave[edge:, block:]
    part_im = wave[:edge, block:] + wave[edge:, :block]
    cos_part, sin_part = spread(twiddle_ref, 0, chan), spread(twiddle_ref, 1, chan)
    turned_re = part_re * cos_part - part_im * sin_part
    turned_im = part_re * sin_part + part_im * cos_part
    high, low = halves(jnp.concatenate([turned_re, turned_im[chan : edge - chan]], 0))
    return dot_three(back_ref[0], back_ref[1], high, low)


def filter_kernel(
    rows, chan, embed_ref, first_bias_ref, freq_ref, inner_ref, second_bias_ref, weight_ref, decay_ref,
    band_ref, into_ref, fourier_ref, twiddle_ref, spec_re_ref, spec_im_ref,
    first_table, second_table, taps_ref, energy_ref, near_ref, far_ref, first_w, second_w, last_w,
):
    block = taps_ref.shape[2]
    hidden = freq_ref.shape[1]
    seq_len = rows * block
    freq = freq_ref[...] * (0.5 / math.pi)
    w_one, w_two, w_three = thirds(embed_ref[...] * freq)
    none = jnp.zeros_like(w_one)
    first_w[:, :hidden] = jnp.concatenate([w_one, w_one, w_one, w_three], 0)
    first_w[:, hidden:] = jnp.concatenate([w_two, w_two, none, none], 0)
    v_one, v_two = halves(inner_ref[...] * freq)
    second_w[:, :hidden] = jnp.concatenate([v_one, v_one], 0)
    second_w[:, hidden:] = jnp.concatenate([v_two, v_two], 0)
    u_one, u_two = halves(weight_ref[...])
    last_w[:, :hidden] = jnp.concatenate([u_one, u_two], 0)
    last_w[:, hidden:] = jnp.concatenate([u_one, jnp.zeros_like(u_two)], 0)
    first_bias = first_bias_ref[...] * freq - 0.25
    second_bias = second_bias_ref[...] * freq - 0.25
    band = band_ref[0:1]
    shift = band_ref[1:2]
    line = band_ref[2:3]
    lag = lax.broadcasted_iota(jnp.int32, (block, 2 * embed_ref.shape[0]), 0).astype(F32)
    turns = lag * band * (1.0 / seq_len)
    first_table[...] = jnp.where(line > 0, 1.0, cos_turns(turns + shift))
    second_table[...] = jnp.where(line > 0, lag * (1.0 / seq_len), cos_turns(turns + (shift + 0.25)))
    start = lax.broadcasted_iota(jnp.int32, (rows, 2 * embed_ref.shape[0]), 0).astype(F32)
    turns = start * band * (1.0 / rows)
    near_ref[...] = jnp.where(line > 0, start * (1.0 / rows), cos_turns(turns))
    far_ref[...] = jnp.where(line > 0, 1.0, cos_turns(turns - 0.25))
    energy_ref[...] = jnp.zeros_like(energy_ref)
    decay = decay_ref[...]
    lanes = lax.broadcasted_iota(jnp.int32, (1, block), 1)
    left = lax.broadcasted_iota(jnp.int32, (1, 2 * embed_ref.shape[0]), 1) < embed_ref.shape[0]
    parts = weight_ref.shape[0]
    is_back = (lax.broadcasted_iota(jnp.int32, (parts, 1), 0) // chan) % 2 == 1

    @pl.loop(0, rows)
    def _(row):
        feature = first_table[...] * near_ref[pl.ds(row, 1), :] + second_table[...] * far_ref[pl.ds(row, 1), :]
        x_one, x_two, x_three = thirds(feature)
        stacked = jnp.concatenate([jnp.where(left, x_one, x_two), jnp.where(left, x_three, x_one)], 1)
        both = dot(stacked, first_w[...])
        layer_one = cos_turns(both[:, :hidden] + both[:, hidden:] + first_bias)
        y_one, y_two = halves(layer_one)
        both = dot(jnp.concatenate([y_one, y_two], 1), second_w[...])
        layer_two = cos_turns(both[:, :hidden] + both[:, hidden:] + second_bias)
        z_one, z_two = halves(layer_two)
        both = lax.dot_general(
            last_w[...], jnp.concatenate([z_one, z_two], 1), (((1,), (1,)), ((), ())), preferred_element_type=F32
        )
        raw = both[:parts] + both[parts:]
        at = lanes + row * block
        taps = raw * jnp.exp(decay * (at.astype(F32) * (-1.0 / seq_len)))
        taps = jnp.where(is_back & (at == 0), 0.0, taps)
        energy_ref[...] += taps * taps
        place = pl.multiple_of(row * chan, chan)
        for k in range(parts // chan):
            taps_ref[k, pl.ds(place, chan), :] = taps[k * chan : (k + 1) * chan]

    total = jnp.sum(energy_ref[...], axis=1, keepdims=True)

    for order in range(parts // (2 * chan)):
        base = order * 2 * chan
        scale = lax.rsqrt(total[base : base + chan] + total[base + chan : base + 2 * chan] + ENERGY_FLOOR)
        scale = jnp.broadcast_to(scale[None], (rows + 1, chan, block)).reshape(-1, block)
        ahead_re, ahead_im = forward(taps_ref[2 * order], into_ref, fourier_ref, twiddle_ref, chan)
        behind_re, behind_im = forward(taps_ref[2 * order + 1], into_ref, fourier_ref, twiddle_ref, chan)
        spec_re_ref[order] = (ahead_re + behind_re) * scale
        spec_im_ref[order] = (ahead_im - behind_im) * scale


def short(signal, taps, first, rows, chan):
    block = signal.shape[1]
    lanes = lax.broadcasted_iota(jnp.int32, signal.shape, 1)
    line = lax.broadcasted_iota(jnp.int32, signal.shape, 0)
    size = signal.shape[0]
    before = pltpu.roll(signal, 1, 1)
    crossed = jnp.where(line < chan, 0.0, pltpu.roll(before, chan, 0))
    before = jnp.where(lanes == 0, crossed, before)
    after = pltpu.roll(signal, block - 1, 1)
    crossed = jnp.where(line >= size - chan, 0.0, pltpu.roll(after, size - chan, 0))
    after = jnp.where(lanes == block - 1, crossed, after)

    def tap(k):
        column = taps[:, first + k : first + k + 1]
        return jnp.broadcast_to(column[None], (rows, chan, block)).reshape(size, block)

    return before * tap(0) + signal * tap(1) + after * tap(2)


def conv_kernel(
    rows, chan, orders, arrived_ref, param_ref, spec_re_ref, spec_im_ref, into_ref, back_ref, fourier_ref,
    twiddle_ref, out_ref,
):
    block = arrived_ref.shape[2]
    size = rows * chan
    param = param_ref[...]

    def signal(k):
        return arrived_ref[:, k * chan : (k + 1) * chan, :].astype(F32).reshape(size, block)

    current = short(signal(0), param, 6, rows, chan)
    for order in range(orders):
        data_re, data_im = forward(current, into_ref, fourier_ref, twiddle_ref, chan)
        spec_re, spec_im = spec_re_ref[order], spec_im_ref[order]
        long_part = backward(
            data_re * spec_re - data_im * spec_im,
            data_re * spec_im + data_im * spec_re,
            back_ref, fourier_ref, twiddle_ref, chan,
        )
        column = param[:, 9 + order : 10 + order]
        skip = jnp.broadcast_to(column[None], (rows, chan, block)).reshape(size, block)
        current = long_part + skip * current
        if order < orders - 1:
            current = current * short(signal(order + 1), param, 3 * order, rows, chan)
    out_ref[...] = current.astype(BF16).reshape(rows, chan, block)


def turn_kernel(first_ref, second_ref, out_ref):
    rows = out_ref.shape[0]
    chan = out_ref.shape[1] // 2
    for k, ref in enumerate((first_ref, second_ref)):
        turned = jnp.transpose(ref[...].astype(F32)).astype(BF16)
        out_ref[:, k * chan : (k + 1) * chan, :] = turned.reshape(rows, chan, -1)


def gate_kernel(mixed_ref, gate_ref, halo_ref, taps_ref, out_ref):
    gate = gate_ref[...].astype(F32)
    block = gate.shape[0]
    line = lax.broadcasted_iota(jnp.int32, gate.shape, 0)
    halo = halo_ref[...].astype(F32)
    taps = taps_ref[...].astype(F32)
    before = jnp.where(line == 0, halo[0:1], pltpu.roll(gate, 1, 0))
    after = jnp.where(line == block - 1, halo[1:2], pltpu.roll(gate, block - 1, 0))
    factor = before * taps[0:1] + gate * taps[1:2] + after * taps[2:3]
    out_ref[...] = (jnp.transpose(mixed_ref[...].astype(F32)) * factor).astype(BF16)


def call(kernel, out_shape, scratch=(), flops=0, moved=0):
    return pl.pallas_call(
        kernel,
        out_shape=out_shape,
        scratch_shapes=scratch,
        cost_estimate=pl.CostEstimate(flops=flops, bytes_accessed=moved, transcendentals=0),
    )


def per_device(
    gate_one, gate_two, values, conv_taps, embed_weight, embed_bias, sine_freq, inner_weight, inner_bias,
    filter_weight, decay_rate, skip_gain, out_weight,
):
    rows = lax.axis_size("row")
    own = lax.axis_index("row")
    block, columns = gate_one.shape
    orders = skip_gain.shape[0]
    chan = columns // rows
    offset = own * chan
    hidden = sine_freq.shape[0]
    features = embed_weight.shape[0]
    bands = (features - 1) // 2
    into, back, fourier, twiddle = tables(rows, chan, block)

    turned = call(turn_kernel, jax.ShapeDtypeStruct((rows, 2 * chan, block), BF16))(values, gate_one)
    arrived = lax.all_to_all(turned, "row", 0, 0, tiled=True)

    down = [(k, k + 1) for k in range(rows - 1)]
    up = [(k + 1, k) for k in range(rows - 1)]
    halo = jnp.concatenate(
        [lax.ppermute(gate_two[-1:], "row", down), lax.ppermute(gate_two[:1], "row", up)], 0
    )

    weight_here = lax.dynamic_slice_in_dim(filter_weight, offset, chan, 3)
    weight_here = jnp.transpose(weight_here.reshape(hidden, -1))
    decay_here = lax.dynamic_slice_in_dim(decay_rate, offset, chan, 2).reshape(-1, 1)
    taps_here = lax.dynamic_slice_in_dim(conv_taps, offset, chan, 2).astype(F32).reshape(-1, chan)
    skip_here = lax.dynamic_slice_in_dim(skip_gain, offset, chan, 1)
    param = jnp.transpose(jnp.concatenate([taps_here, skip_here], 0))

    width = 64
    embed = jnp.pad(embed_weight, ((0, width - features), (0, 0)))
    steps = np.linspace(0.0001, bands - 1, bands).astype(np.float32)
    band = np.zeros((3, width), np.float32)
    band[0, 1:features] = np.concatenate([steps, steps])
    band[1, 1 + bands : features] = 0.25
    band[2, 0] = 1
    band[:, features:] = 0
    band = np.concatenate([band, band], 1)

    edge = (rows + 1) * chan
    parts = weight_here.shape[0]
    spec_shape = jax.ShapeDtypeStruct((orders, edge, block), F32)
    spec_re, spec_im = call(
        functools.partial(filter_kernel, rows, chan),
        (spec_shape, spec_shape),
        (
            pltpu.VMEM((block, 2 * width), F32),
            pltpu.VMEM((block, 2 * width), F32),
            pltpu.VMEM((parts // chan, rows * chan, block), F32),
            pltpu.VMEM((parts, block), F32),
            pltpu.VMEM((rows, 2 * width), F32),
            pltpu.VMEM((rows, 2 * width), F32),
            pltpu.VMEM((4 * width, 2 * hidden), BF16),
            pltpu.VMEM((2 * hidden, 2 * hidden), BF16),
            pltpu.VMEM((2 * parts, 2 * hidden), BF16),
        ),
        flops=12_000_000_000,
    )(
        embed, embed_bias[None], sine_freq[None], inner_weight, inner_bias[None], weight_here, decay_here,
        band, into, fourier, twiddle,
    )
    mixed = call(
        functools.partial(conv_kernel, rows, chan, orders),
        jax.ShapeDtypeStruct((rows, chan, block), BF16),
        flops=5_000_000_000,
    )(arrived, param, spec_re, spec_im, into, back, fourier, twiddle)
    mixed = lax.all_to_all(mixed, "row", 0, 0, tiled=True).reshape(columns, block)
    gated = call(gate_kernel, jax.ShapeDtypeStruct((block, columns), BF16))(mixed, gate_two, halo, conv_taps[1])
    return finish(gated, out_weight)


def finish(gated, out_weight):
    peers = lax.axis_size("col")
    block, columns = gated.shape
    half = block // 2
    upper = lax.all_gather(gated[:half], "col", axis=0)
    lower = lax.all_gather(gated[half:], "col", axis=0)
    weight = out_weight.reshape(peers, columns, -1)
    return jnp.concatenate(
        [
            jnp.einsum("crk,ckn->rn", part, weight, preferred_element_type=F32).astype(BF16)
            for part in (upper, lower)
        ],
        0,
    )


def solution(mesh):
    spread_rows = ("grp", "row")
    in_specs = (
        P(spread_rows, "col"),
        P(spread_rows, "col"),
        P(spread_rows, "col"),
        P(None, None, "col"),
        P(),
        P(),
        P(),
        P(),
        P(),
        P(None, None, None, "col"),
        P(None, None, "col"),
        P(None, "col"),
        P(None, "col"),
    )
    return jax.shard_map(
        per_device, mesh=mesh, in_specs=in_specs, out_specs=P(spread_rows, "col"), check_vma=False
    )
```

profile of v0, /device:TPU:80, one launch (start us, length us, event | category | flops | bytes accessed | tf_op | source)
XLA Modules:
  0.0 172.4 jit_solution(11155737946349139133)
XLA Ops:
  0.0 2.0 %shard_map.172 = bf16[32,16,256]{2,1,0:T(8,128)(2,1)} custom-call(bf16[256,256]{1,0:T(8,128)(2,1)} %first_ref.1, bf16[256,256]{1,0:T(8,128)(2,1)} %second_ref.1), custom_call_target="tpu_custom_call" | custom-call | tf_op jit(solution)/shard_map/pallas_call | solution.py:279
  2.0 44.4 %all-to-all-start = ((bf16[32,16,256]{2,1,0:T(8,128)(2,1)}), bf16[32,16,256]{2,1,0:T(8,128)(2,1)S(1)}, u32[]{:S(2)}, u32[]{:S(2)}) async-start(bf16[32,16,256]{2,1,0:T(8,128)(2,1)} %shard_map.172), calls=%async_computation | async-start | bytes 524288 | tf_op jit(solution)/shard_map/all_to_all | solution.py:280
  46.4 0.8 constant_dynamic-slice_fusion.2
  47.3 0.8 dynamic-slice_convert_fusion
  48.1 1.3 constant_dynamic-slice_fusion.1
  49.4 0.8 copy.25
  50.2 0.8 constant_dynamic-slice_fusion
  50.9 0.7 reshape.30.decay_ref
  51.6 0.7 maximum_bitcast_fusion.param_ref
  52.3 1.3 pad.4.embed_ref
  53.6 23.2 %shard_map.173 = (f32[2,264,256]{2,1,0:T(8,128)}, f32[2,264,256]{2,1,0:T(8,128)}) custom-call(f32[64,128]{1,0:T(8,128)} %pad.4.embed_ref, f32[1,128]{1,0:T(1,128)} %bitcast.32, f32[1,128]{1,0:T(1,128)} %bitcast.33, f32[128,128]{1,0:T(8,128)} %inner_ref.1, f32[1,128]{1,0:T(1,128)} %bitcast.34, f32[32,128]{1,0:T(8,128)} %bitcast.31, ...), custom_call_target="tpu_custom_call" | custom-call | flops 12000000000 | tf_op jit(solution)/shard_map/pallas_call | solution.py:308
  76.8 0.7 copy-done.2
  77.5 8.4 %shard_map.174 = bf16[32,8,256]{2,1,0:T(8,128)(2,1)} custom-call(bf16[32,16,256]{2,1,0:T(8,128)(2,1)} %copy-done.2, f32[8,11]{1,0:T(8,128)} %maximum_bitcast_fusion.param_ref, f32[2,264,256]{2,1,0:T(8,128)} %get-tuple-element.7.spec_re_ref, f32[2,264,256]{2,1,0:T(8,128)} %get-tuple-element.8.spec_im_ref, bf16[2,512,256]{2,1,0:T(8,128)(2,1)} %constant.25.clone.into_ref, ...), custom_call_target="tpu_custom_call" | custom-call | flops 5000000000 | tf_op jit(solution)/shard_map/pallas_call | solution.py:327
  86.0 12.4 %all-to-all-start.1 = ((bf16[32,8,256]{2,1,0:T(8,128)(2,1)}), bf16[32,8,256]{2,1,0:T(8,128)(2,1)S(1)}, u32[]{:S(2)}, u32[]{:S(2)}) async-start(bf16[32,8,256]{2,1,0:T(8,128)(2,1)} %shard_map.174), calls=%async_computation.1 | async-start | bytes 262144 | tf_op jit(solution)/shard_map/all_to_all | solution.py:332
  98.4 0.7 fusion.3
  99.1 1.3 collective-permute-start.1
  100.4 3.1 %collective-permute-start = (bf16[1,256]{1,0:T(2,128)(2,1)S(1)}, bf16[1,256]{1,0:T(2,128)(2,1)S(1)}, u32[]{:S(2)}, u32[]{:S(2)}) collective-permute-start(bf16[1,256]{1,0:T(2,128)(2,1)S(1)} %get-tuple-element.11), channel_id=1, source_target_pairs={{0,8},{8,16},{16,24},{24,32},{32,40},{40,48},{48,56},{56,64},{64,7... | collective-permute-start | bytes 1544 | tf_op jit(solution)/shard_map/ppermute | solution.py:285
  103.5 1.3 slice_bitcast_fusion.taps_ref
  105.4 9.5 %all-to-all-done.1 = bf16[32,8,256]{2,1,0:T(8,128)(2,1)S(1)} async-done(((bf16[32,8,256]{2,1,0:T(8,128)(2,1)}), bf16[32,8,256]{2,1,0:T(8,128)(2,1)S(1)}, u32[]{:S(2)}, u32[]{:S(2)}) %all-to-all-start.1) | async-done | bytes 131104 | tf_op jit(solution)/shard_map/all_to_all | solution.py:332
  115.5 1.7 %shard_map.175 = bf16[256,256]{1,0:T(8,128)(2,1)} custom-call(bf16[256,256]{1,0:T(8,128)(2,1)} %bitcast.30, bf16[256,256]{1,0:T(8,128)(2,1)} %gate_ref.1, bf16[2,256]{1,0:T(2,128)(2,1)} %pad_maximum_fusion.1.halo_ref, bf16[3,256]{1,0:T(4,128)(2,1)} %slice_bitcast_fusion.taps_ref), custom_call_target="tpu_custom_call" | custom-call | tf_op jit(solution)/shard_map/pallas_call | solution.py:333
  117.3 0.9 fusion.2
  118.2 27.3 %all-gather.1 = bf16[1024,256]{1,0:T(8,128)(2,1)S(1)} all-gather(bf16[128,256]{1,0:T(8,128)(2,1)S(1)} %get-tuple-element.10), channel_id=3, replica_groups=mesh['grp'=2,'row'=32,'col'=8] {'col'}, dimensions={0}, use_global_device_ids=true | all-gather | bytes 589824 | tf_op jit(solution)/shard_map/all_gather | solution.py:342
  145.5 25.3 %all-gather = bf16[1024,256]{1,0:T(8,128)(2,1)S(1)} all-gather(bf16[128,256]{1,0:T(8,128)(2,1)S(1)} %get-tuple-element.9), channel_id=2, replica_groups=mesh['grp'=2,'row'=32,'col'=8] {'col'}, dimensions={0}, use_global_device_ids=true | all-gather | bytes 589824 | tf_op jit(solution)/shard_map/all_gather | solution.py:341
  171.6 0.7 pad_maximum_fusion
  (14 shorter events, 2.3 us)
Async XLA Ops:
  0.0 170.7 %copy-start = (bf16[2048,512]{1,0:T(8,128)(2,1)S(1)}, bf16[2048,512]{1,0:T(8,128)(2,1)}, u32[]{:S(2)}) copy-start(bf16[2048,512]{1,0:T(8,128)(2,1)} %param.30) | copy-start | bytes 6291460
  2.0 74.9 %all-to-all-start = ((bf16[32,16,256]{2,1,0:T(8,128)(2,1)}), bf16[32,16,256]{2,1,0:T(8,128)(2,1)S(1)}, u32[]{:S(2)}, u32[]{:S(2)}) async-start(bf16[32,16,256]{2,1,0:T(8,128)(2,1)} %shard_map.172), calls=%async_computation | async-start | bytes 524288 | tf_op jit(solution)/shard_map/all_to_all | solution.py:280
  76.8 0.7 copy-start.2
  86.0 28.9 %all-to-all-start.1 = ((bf16[32,8,256]{2,1,0:T(8,128)(2,1)}), bf16[32,8,256]{2,1,0:T(8,128)(2,1)S(1)}, u32[]{:S(2)}, u32[]{:S(2)}) async-start(bf16[32,8,256]{2,1,0:T(8,128)(2,1)} %shard_map.174), calls=%async_computation.1 | async-start | bytes 262144 | tf_op jit(solution)/shard_map/all_to_all | solution.py:332
  99.1 5.7 %collective-permute-start.1 = (bf16[1,256]{1,0:T(2,128)(2,1)S(1)}, bf16[1,256]{1,0:T(2,128)(2,1)S(1)}, u32[]{:S(2)}, u32[]{:S(2)}) collective-permute-start(bf16[1,256]{1,0:T(2,128)(2,1)S(1)} %get-tuple-element.12), channel_id=1, source_target_pairs={{8,0},{16,8},{24,16},{32,24},{40,32},{48,40},{56,48},{64,56},{72,6... | collective-permute-start | bytes 1544 | tf_op jit(solution)/shard_map/ppermute | solution.py:285
  100.4 4.4 %collective-permute-start = (bf16[1,256]{1,0:T(2,128)(2,1)S(1)}, bf16[1,256]{1,0:T(2,128)(2,1)S(1)}, u32[]{:S(2)}, u32[]{:S(2)}) collective-permute-start(bf16[1,256]{1,0:T(2,128)(2,1)S(1)} %get-tuple-element.11), channel_id=1, source_target_pairs={{0,8},{8,16},{16,24},{24,32},{32,40},{40,48},{48,56},{56,64},{64,7... | collective-permute-start | bytes 1544 | tf_op jit(solution)/shard_map/ppermute | solution.py:285
  114.9 0.7 copy-start.1
where the time goes:
time: 173 us; the launch traced here: 172 us
  starting transfers between devices  61.2 us (35%)
  blocking collectives  52.6 us (30%)
  Pallas kernels  35.3 us (20%)
  local copies, waits for them, and re-layouts  9.97 us (6%)
  waiting for transfers between devices  9.53 us (6%)
  other arithmetic  2.74 us (2%)
    all_to_all x1, starting transfers between devices, per_device(): arrived = lax.all_to_all(turned, 'row', 0, 0, tiled=True)  44.4 us
    all_gather x1, blocking collectives, finish(): lower = lax.all_gather(gated[half:], 'col', axis=0)  27.3 us
    all_gather x1, blocking collectives, finish(): upper = lax.all_gather(gated[:half], 'col', axis=0)  25.3 us
    pallas_call x1, Pallas kernels, per_device(): call(functools.partial(filter_kernel, rows, chan), (spec_shape, spec_shap...  23.2 us
    all_to_all x1, starting transfers between devices, per_device(): lax.all_to_all(mixed, 'row', 0, 0, tiled=True).reshape(columns, block)  12.4 us
    all_to_all x1, waiting for transfers between devices, per_device(): lax.all_to_all(mixed, 'row', 0, 0, tiled=True).reshape(columns, block)  9.52 us
    pallas_call x1, Pallas kernels, per_device(): call(functools.partial(conv_kernel, rows, chan, orders), jax.ShapeDtypeSt...  8.42 us
  transfers between devices with their start and end apart: 4, of which 1 were waited for; matrix products, arithmetic and copies ran while one was open for 6% of the time, Pallas kernels for 13%

commit v1 on v0

--- a/solution.py
+++ b/solution.py
@@ -19,19 +19,15 @@
     return high, (value - high.astype(F32)).astype(BF16)
 
 
-def thirds(value):
-    high = value.astype(BF16)
-    rest = value - high.astype(F32)
-    middle = rest.astype(BF16)
-    return high, middle, (rest - middle.astype(F32)).astype(BF16)
-
-
 def dot(left, right):
     return jnp.dot(left, right, preferred_element_type=F32)
 
 
-def dot_three(left_high, left_low, right_high, right_low):
-    return dot(left_high, right_high) + dot(left_low, right_high) + dot(left_high, right_low)
+def dot_wide(left_high, left_low, right_high, right_low):
+    return dot(
+        jnp.concatenate([left_high, left_low, left_high], 1),
+        jnp.concatenate([right_high, right_high, right_low], 0),
+    )
 
 
 def cos_turns(turns):
@@ -46,7 +42,7 @@
 
 def fit_sine():
     nodes = 0.25 * np.cos(np.pi * (np.arange(64) + 0.5) / 128)
-    powers = np.stack([nodes ** (2 * i + 1) for i in range(6)], 1)
+    powers = np.stack([nodes ** (2 * i + 1) for i in range(5)], 1)
     return [float(v) for v in np.linalg.lstsq(powers, -np.sin(2 * np.pi * nodes), rcond=None)[0]]
 
 
@@ -70,10 +66,10 @@
         [np.kron(weight * np.cos(phase), eye), np.kron(-(weight * np.sin(phase))[1:-1], eye)]
     ).T
     inner = 2 * np.pi * (np.arange(block)[:, None] * np.arange(block)[None] % block) / block
-    fourier = np.concatenate([np.cos(inner), np.sin(inner)], 1)
+    pair = np.concatenate([np.cos(inner), np.sin(inner)], 0)
     turn = 2 * np.pi * half[:, None] * np.arange(block)[None] / (waves * block)
     twiddle = np.stack([np.cos(turn), np.sin(turn)]).astype(np.float32)
-    return split_constant(into), split_constant(back), split_constant(fourier), twiddle
+    return split_constant(into), split_constant(back), split_constant(pair), twiddle
 
 
 def spread(twiddle_ref, part, chan):
@@ -81,49 +77,62 @@
     return jnp.broadcast_to(value[:, None, :], (value.shape[0], chan, value.shape[1])).reshape(-1, value.shape[1])
 
 
-def forward(field, into_ref, fourier_ref, twiddle_ref, chan):
-    block = field.shape[1]
+def first_stage(field, into_ref, chan):
     edge = field.shape[0] + chan
     high, low = halves(field)
-    mixed = dot_three(into_ref[0], into_ref[1], high, low)
-    zero = jnp.zeros((chan, block), F32)
-    part_re = mixed[:edge]
-    part_im = jnp.concatenate([zero, mixed[edge:], zero], 0)
-    cos_part, sin_part = spread(twiddle_ref, 0, chan), spread(twiddle_ref, 1, chan)
-    turned = jnp.concatenate(
-        [part_re * cos_part + part_im * sin_part, part_im * cos_part - part_re * sin_part], 0
-    )
-    high, low = halves(turned)
-    wave = dot_three(high, low, fourier_ref[0], fourier_ref[1])
-    return wave[:edge, :block] + wave[edge:, block:], wave[edge:, :block] - wave[:edge, block:]
-
-
-def backward(part_re, part_im, back_ref, fourier_ref, twiddle_ref, chan):
-    edge, block = part_re.shape
-    high, low = halves(jnp.concatenate([part_re, part_im], 0))
-    wave = dot_three(high, low, fourier_ref[0], fourier_ref[1])
-    part_re = wave[:edge, :block] - wave[edge:, block:]
-    part_im = wave[:edge, block:] + wave[edge:, :block]
-    cos_part, sin_part = spread(twiddle_ref, 0, chan), spread(twiddle_ref, 1, chan)
-    turned_re = part_re * cos_part - part_im * sin_part
-    turned_im = part_re * sin_part + part_im * cos_part
+    part_re = dot_wide(into_ref[0, :edge], into_ref[1, :edge], high, low)
+    part_im = dot_wide(into_ref[0, edge:], into_ref[1, edge:], high, low)
+    zero = jnp.zeros((chan, field.shape[1]), F32)
+    return part_re, jnp.concatenate([zero, part_im, zero], 0)
+
+
+def pair_product(first, second, pair_ref):
+    first_high, first_low = halves(first)
+    second_high, second_low = halves(second)
+    return dot_wide(
+        jnp.concatenate([first_high, second_high], 1),
+        jnp.concatenate([first_low, second_low], 1),
+        pair_ref[0],
+        pair_ref[1],
+    )
+
+
+def forward(field, into_ref, pair_ref, cos_part, sin_part, chan):
+    part_re, part_im = first_stage(field, into_ref, chan)
+    turned_re = part_re * cos_part + part_im * sin_part
+    turned_im = part_im * cos_part - part_re * sin_part
+    return pair_product(turned_re, turned_im, pair_ref), pair_product(turned_im, -turned_re, pair_ref)
+
+
+def backward(part_re, part_im, back_ref, pair_ref, cos_part, sin_part, chan):
+    edge = part_re.shape[0]
+    wave_re = pair_product(part_re, -part_im, pair_ref)
+    wave_im = pair_product(part_im, part_re, pair_ref)
+    turned_re = wave_re * cos_part - wave_im * sin_part
+    turned_im = wave_re * sin_part + wave_im * cos_part
     high, low = halves(jnp.concatenate([turned_re, turned_im[chan : edge - chan]], 0))
-    return dot_three(back_ref[0], back_ref[1], high, low)
+    middle = back_ref.shape[1] // 2
+    return jnp.concatenate(
+        [
+            dot_wide(back_ref[0, :middle], back_ref[1, :middle], high, low),
+            dot_wide(back_ref[0, middle:], back_ref[1, middle:], high, low),
+        ],
+        0,
+    )
 
 
 def filter_kernel(
     rows, chan, embed_ref, first_bias_ref, freq_ref, inner_ref, second_bias_ref, weight_ref, decay_ref,
-    band_ref, into_ref, fourier_ref, twiddle_ref, spec_re_ref, spec_im_ref,
+    band_ref, into_ref, pair_ref, twiddle_ref, spec_re_ref, spec_im_ref,
     first_table, second_table, taps_ref, energy_ref, near_ref, far_ref, first_w, second_w, last_w,
 ):
     block = taps_ref.shape[2]
     hidden = freq_ref.shape[1]
     seq_len = rows * block
     freq = freq_ref[...] * (0.5 / math.pi)
-    w_one, w_two, w_three = thirds(embed_ref[...] * freq)
-    none = jnp.zeros_like(w_one)
-    first_w[:, :hidden] = jnp.concatenate([w_one, w_one, w_one, w_three], 0)
-    first_w[:, hidden:] = jnp.concatenate([w_two, w_two, none, none], 0)
+    w_one, w_two = halves(embed_ref[...] * freq)
+    first_w[:, :hidden] = jnp.concatenate([w_one, w_one], 0)
+    first_w[:, hidden:] = jnp.concatenate([w_two, w_two], 0)
     v_one, v_two = halves(inner_ref[...] * freq)
     second_w[:, :hidden] = jnp.concatenate([v_one, v_one], 0)
     second_w[:, hidden:] = jnp.concatenate([v_two, v_two], 0)
@@ -150,12 +159,10 @@
     parts = weight_ref.shape[0]
     is_back = (lax.broadcasted_iota(jnp.int32, (parts, 1), 0) // chan) % 2 == 1
 
-    @pl.loop(0, rows)
-    def _(row):
+    def lags(row):
         feature = first_table[...] * near_ref[pl.ds(row, 1), :] + second_table[...] * far_ref[pl.ds(row, 1), :]
-        x_one, x_two, x_three = thirds(feature)
-        stacked = jnp.concatenate([jnp.where(left, x_one, x_two), jnp.where(left, x_three, x_one)], 1)
-        both = dot(stacked, first_w[...])
+        x_one, x_two = halves(feature)
+        both = dot(jnp.where(left, x_one, x_two), first_w[...])
         layer_one = cos_turns(both[:, :hidden] + both[:, hidden:] + first_bias)
         y_one, y_two = halves(layer_one)
         both = dot(jnp.concatenate([y_one, y_two], 1), second_w[...])
@@ -167,22 +174,35 @@
         raw = both[:parts] + both[parts:]
         at = lanes + row * block
         taps = raw * jnp.exp(decay * (at.astype(F32) * (-1.0 / seq_len)))
-        taps = jnp.where(is_back & (at == 0), 0.0, taps)
-        energy_ref[...] += taps * taps
-        place = pl.multiple_of(row * chan, chan)
-        for k in range(parts // chan):
-            taps_ref[k, pl.ds(place, chan), :] = taps[k * chan : (k + 1) * chan]
+        return jnp.where(is_back & (at == 0), 0.0, taps)
+
+    @pl.loop(0, rows // 2)
+    def _(step):
+        found = [lags(2 * step + k) for k in range(2)]
+        energy_ref[...] += found[0] * found[0] + found[1] * found[1]
+        for k in range(2):
+            place = pl.multiple_of((2 * step + k) * chan, chan)
+            for order in range(parts // (2 * chan)):
+                base = order * 2 * chan
+                ahead = found[k][base : base + chan]
+                behind = found[k][base + chan : base + 2 * chan]
+                taps_ref[2 * order, pl.ds(place, chan), :] = ahead + behind
+                taps_ref[2 * order + 1, pl.ds(place, chan), :] = ahead - behind
 
     total = jnp.sum(energy_ref[...], axis=1, keepdims=True)
-
+    cos_part, sin_part = spread(twiddle_ref, 0, chan), spread(twiddle_ref, 1, chan)
     for order in range(parts // (2 * chan)):
         base = order * 2 * chan
         scale = lax.rsqrt(total[base : base + chan] + total[base + chan : base + 2 * chan] + ENERGY_FLOOR)
         scale = jnp.broadcast_to(scale[None], (rows + 1, chan, block)).reshape(-1, block)
-        ahead_re, ahead_im = forward(taps_ref[2 * order], into_ref, fourier_ref, twiddle_ref, chan)
-        behind_re, behind_im = forward(taps_ref[2 * order + 1], into_ref, fourier_ref, twiddle_ref, chan)
-        spec_re_ref[order] = (ahead_re + behind_re) * scale
-        spec_im_ref[order] = (ahead_im - behind_im) * scale
+        even_re, even_im = first_stage(taps_ref[2 * order], into_ref, chan)
+        odd_re, odd_im = first_stage(taps_ref[2 * order + 1], into_ref, chan)
+        spec_re_ref[order] = scale * pair_product(
+            even_re * cos_part + even_im * sin_part, even_im * cos_part - even_re * sin_part, pair_ref
+        )
+        spec_im_ref[order] = scale * pair_product(
+            odd_im * cos_part - odd_re * sin_part, -(odd_re * cos_part + odd_im * sin_part), pair_ref
+        )
 
 
 def short(signal, taps, first, rows, chan):
@@ -205,7 +225,7 @@
 
 
 def conv_kernel(
-    rows, chan, orders, arrived_ref, param_ref, spec_re_ref, spec_im_ref, into_ref, back_ref, fourier_ref,
+    rows, chan, orders, arrived_ref, param_ref, spec_re_ref, spec_im_ref, into_ref, back_ref, pair_ref,
     twiddle_ref, out_ref,
 ):
     block = arrived_ref.shape[2]
@@ -215,14 +235,15 @@
     def signal(k):
         return arrived_ref[:, k * chan : (k + 1) * chan, :].astype(F32).reshape(size, block)
 
+    cos_part, sin_part = spread(twiddle_ref, 0, chan), spread(twiddle_ref, 1, chan)
     current = short(signal(0), param, 6, rows, chan)
     for order in range(orders):
-        data_re, data_im = forward(current, into_ref, fourier_ref, twiddle_ref, chan)
+        data_re, data_im = forward(current, into_ref, pair_ref, cos_part, sin_part, chan)
         spec_re, spec_im = spec_re_ref[order], spec_im_ref[order]
         long_part = backward(
             data_re * spec_re - data_im * spec_im,
             data_re * spec_im + data_im * spec_re,
-            back_ref, fourier_ref, twiddle_ref, chan,
+            back_ref, pair_ref, cos_part, sin_part, chan,
         )
         column = param[:, 9 + order : 10 + order]
         skip = jnp.broadcast_to(column[None], (rows, chan, block)).reshape(size, block)
@@ -249,15 +270,18 @@
     before = jnp.where(line == 0, halo[0:1], pltpu.roll(gate, 1, 0))
     after = jnp.where(line == block - 1, halo[1:2], pltpu.roll(gate, block - 1, 0))
     factor = before * taps[0:1] + gate * taps[1:2] + after * taps[2:3]
-    out_ref[...] = (jnp.transpose(mixed_ref[...].astype(F32)) * factor).astype(BF16)
-
-
-def call(kernel, out_shape, scratch=(), flops=0, moved=0):
+    gated = (jnp.transpose(mixed_ref[...].astype(F32)) * factor).astype(BF16)
+    for peer in range(out_ref.shape[0]):
+        out_ref[peer] = gated
+
+
+def call(kernel, out_shape, scratch=(), flops=0, limit=12):
     return pl.pallas_call(
         kernel,
         out_shape=out_shape,
         scratch_shapes=scratch,
-        cost_estimate=pl.CostEstimate(flops=flops, bytes_accessed=moved, transcendentals=0),
+        cost_estimate=pl.CostEstimate(flops=flops, bytes_accessed=0, transcendentals=0),
+        compiler_params=pltpu.CompilerParams(vmem_limit_bytes=limit << 20),
     )
 
 
@@ -273,8 +297,9 @@
     offset = own * chan
     hidden = sine_freq.shape[0]
     features = embed_weight.shape[0]
+    peers = lax.axis_size("col")
     bands = (features - 1) // 2
-    into, back, fourier, twiddle = tables(rows, chan, block)
+    into, back, pair, twiddle = tables(rows, chan, block)
 
     turned = call(turn_kernel, jax.ShapeDtypeStruct((rows, 2 * chan, block), BF16))(values, gate_one)
     arrived = lax.all_to_all(turned, "row", 0, 0, tiled=True)
@@ -315,39 +340,34 @@
             pltpu.VMEM((parts, block), F32),
             pltpu.VMEM((rows, 2 * width), F32),
             pltpu.VMEM((rows, 2 * width), F32),
-            pltpu.VMEM((4 * width, 2 * hidden), BF16),
+            pltpu.VMEM((2 * width, 2 * hidden), BF16),
             pltpu.VMEM((2 * hidden, 2 * hidden), BF16),
             pltpu.VMEM((2 * parts, 2 * hidden), BF16),
         ),
         flops=12_000_000_000,
+        limit=20,
     )(
         embed, embed_bias[None], sine_freq[None], inner_weight, inner_bias[None], weight_here, decay_here,
-        band, into, fourier, twiddle,
+        band, into, pair, twiddle,
     )
     mixed = call(
         functools.partial(conv_kernel, rows, chan, orders),
         jax.ShapeDtypeStruct((rows, chan, block), BF16),
         flops=5_000_000_000,
-    )(arrived, param, spec_re, spec_im, into, back, fourier, twiddle)
+        limit=20,
+    )(arrived, param, spec_re, spec_im, into, back, pair, twiddle)
     mixed = lax.all_to_all(mixed, "row", 0, 0, tiled=True).reshape(columns, block)
-    gated = call(gate_kernel, jax.ShapeDtypeStruct((block, columns), BF16))(mixed, gate_two, halo, conv_taps[1])
+    gated = call(gate_kernel, jax.ShapeDtypeStruct((peers, block, columns), BF16), limit=12)(
+        mixed, gate_two, halo, conv_taps[1]
+    )
     return finish(gated, out_weight)
 
 
 def finish(gated, out_weight):
-    peers = lax.axis_size("col")
-    block, columns = gated.shape
-    half = block // 2
-    upper = lax.all_gather(gated[:half], "col", axis=0)
-    lower = lax.all_gather(gated[half:], "col", axis=0)
+    peers, block, columns = gated.shape
+    everyone = lax.all_to_all(gated, "col", 0, 0, tiled=True)
     weight = out_weight.reshape(peers, columns, -1)
-    return jnp.concatenate(
-        [
-            jnp.einsum("crk,ckn->rn", part, weight, preferred_element_type=F32).astype(BF16)
-            for part in (upper, lower)
-        ],
-        0,
-    )
+    return jnp.einsum("crk,ckn->rn", everyone, weight, preferred_element_type=F32).astype(BF16)
 
 
 def solution(mesh):

time: 173 us -> 152 us (0.88)
  blocking collectives: 52.6 us -> 34.9 us
  Pallas kernels: 35.3 us -> 22.1 us
  local copies, waits for them, and re-layouts: 9.97 us -> 18.7 us
  waiting for transfers between devices: 9.53 us -> 12.7 us
  other arithmetic: 2.74 us -> 0.84 us
    all_gather x2 -> x0, blocking collectives: 52.6 us -> none  [the longest x1 27.3 us: finish(): lower = lax.all_gather(gated[half:], 'col', axis=0)]
    all_to_all x0 -> x1, blocking collectives: none -> 34.9 us  [finish(): everyone = lax.all_to_all(gated, 'col', 0, 0, tiled=True)]
    unnamed x7 -> x41, local copies, waits for them, and re-layouts: 1.44 us -> 14.1 us
    pallas_call x1, Pallas kernels: 23.2 us -> 16.7 us  [per_device(): call(functools.partial(filter_kernel, rows, chan), (spec_shape, spec_shap...]
    pallas_call x1, Pallas kernels: 8.42 us -> 4.38 us  [per_device(): call(functools.partial(conv_kernel, rows, chan, orders), jax.ShapeDtypeSt...]
    ppermute x1, waiting for transfers between devices: 0.01 us -> 2.22 us  [per_device(): lax.ppermute(gate_two[:1], 'row', up)]
  transfers between devices with their start and end apart: 4 -> 4, of which waited for: 1 -> 2; matrix products, arithmetic and copies ran while one was open for 6% -> 4% of each run, Pallas kernels for 13% -> 11%
where the time goes in v1:
time: 152 us; the launch traced here: 151 us
  starting transfers between devices  59.9 us (39%)
  blocking collectives  34.9 us (23%)
  Pallas kernels  22.1 us (15%)
  local copies, waits for them, and re-layouts  18.7 us (12%)
  waiting for transfers between devices  12.7 us (8%)
    all_to_all x1, starting transfers between devices, per_device(): arrived = lax.all_to_all(turned, 'row', 0, 0, tiled=True)  44.4 us
    all_to_all x1, blocking collectives, finish(): everyone = lax.all_to_all(gated, 'col', 0, 0, tiled=True)  34.9 us
    pallas_call x1, Pallas kernels, per_device(): call(functools.partial(filter_kernel, rows, chan), (spec_shape, spec_shap...  16.7 us
    unnamed x41, local copies, waits for them, and re-layouts  14.1 us
    all_to_all x1, starting transfers between devices, per_device(): lax.all_to_all(mixed, 'row', 0, 0, tiled=True).reshape(columns, block)  12.4 us
    all_to_all x1, waiting for transfers between devices, per_device(): lax.all_to_all(mixed, 'row', 0, 0, tiled=True).reshape(columns, block)  10.5 us
    pallas_call x1, Pallas kernels, per_device(): call(functools.partial(conv_kernel, rows, chan, orders), jax.ShapeDtypeSt...  4.38 us
  transfers between devices with their start and end apart: 4, of which 2 were waited for; matrix products, arithmetic and copies ran while one was open for 4% of the time, Pallas kernels for 11%

profile of v1, /device:TPU:80, one launch (start us, length us, event | category | flops | bytes accessed | tf_op | source)
XLA Modules:
  0.0 150.6 jit_solution(8759124830720968446)
XLA Ops:
  0.0 1.1 copy-done.2
  1.1 0.9 copy-done.3
  2.0 0.8 shard_map.172
  2.8 44.4 %all-to-all-start = ((bf16[32,16,256]{2,1,0:T(8,128)(2,1)}), bf16[32,16,256]{2,1,0:T(8,128)(2,1)S(1)}, u32[]{:S(2)}, u32[]{:S(2)}) async-start(bf16[32,16,256]{2,1,0:T(8,128)(2,1)} %shard_map.172), calls=%async_computation | async-start | bytes 524288 | tf_op jit(solution)/shard_map/all_to_all | solution.py:305
  49.8 1.3 constant_dynamic-slice_fusion.1
  52.0 0.8 copy-done.4
  54.8 1.0 copy-done.8
  55.9 1.0 copy-done.10
  56.9 0.9 copy-done.13
  58.5 16.7 %shard_map.173 = (f32[2,264,256]{2,1,0:T(8,128)S(1)}, f32[2,264,256]{2,1,0:T(8,128)S(1)}) custom-call(f32[64,128]{1,0:T(8,128)S(1)} %pad.4.embed_ref, f32[1,128]{1,0:T(1,128)S(1)} %bitcast.21, f32[1,128]{1,0:T(1,128)S(1)} %bitcast.22, f32[128,128]{1,0:T(8,128)S(1)} %copy-done.4, f32[1,128]{1,0:T(1,128)S(1)} %bitcast.23, f32[32,128]{1,0:T(8,128)S(1)} %bitcast.20, ...), custom_call_target="tpu_custom_call" | custom-call | flops 12000000000 | tf_op jit(solution)/shard_map/pallas_call | solution.py:333
  75.2 0.8 copy-done.16
  76.0 0.8 copy-done.18
  76.8 1.0 copy-done.12
  77.9 0.9 copy-done.14
  78.8 1.0 copy-done.17
  79.8 1.0 copy-done.19
  80.9 4.4 %shard_map.174 = bf16[32,8,256]{2,1,0:T(8,128)(2,1)} custom-call(bf16[32,16,256]{2,1,0:T(8,128)(2,1)S(1)} %all-to-all-done.arrived_ref, f32[8,11]{1,0:T(8,128)S(1)} %maximum_bitcast_fusion.param_ref, f32[2,264,256]{2,1,0:T(8,128)S(1)} %copy-done.17, f32[2,264,256]{2,1,0:T(8,128)S(1)} %copy-done.19, bf16[2,512,256]{2,1,0:T(8,128)(2,1)S(1)} %copy-done.11, ...), custom_call_target="tpu_custom_call" | custom-call | flops 5000000000 | tf_op jit(solution)/shard_map/pallas_call | solution.py:353
  85.2 12.4 %all-to-all-start.1 = ((bf16[32,8,256]{2,1,0:T(8,128)(2,1)}), bf16[32,8,256]{2,1,0:T(8,128)(2,1)S(1)}, u32[]{:S(2)}, u32[]{:S(2)}) async-start(bf16[32,8,256]{2,1,0:T(8,128)(2,1)} %shard_map.174), calls=%async_computation.1 | async-start | bytes 262144 | tf_op jit(solution)/shard_map/all_to_all | solution.py:359
  97.7 1.7 %collective-permute-start = (bf16[1,256]{1,0:T(2,128)(2,1)S(1)}, bf16[1,256]{1,0:T(2,128)(2,1)S(1)}, u32[]{:S(2)}, u32[]{:S(2)}) collective-permute-start(bf16[1,256]{1,0:T(2,128)(2,1)S(1)} %get-tuple-element.9), channel_id=1, source_target_pairs={{0,8},{8,16},{16,24},{24,32},{32,40},{40,48},{48,56},{56,64},{64,7... | collective-permute-start | bytes 1544 | tf_op jit(solution)/shard_map/ppermute | solution.py:310
  99.4 1.3 collective-permute-start.1
  101.4 2.2 %collective-permute-done.1 = bf16[1,256]{1,0:T(2,128)(2,1)S(1)} collective-permute-done((bf16[1,256]{1,0:T(2,128)(2,1)S(1)}, bf16[1,256]{1,0:T(2,128)(2,1)S(1)}, u32[]{:S(2)}, u32[]{:S(2)}) %collective-permute-start.1) | collective-permute-done | bytes 544 | tf_op jit(solution)/shard_map/ppermute | solution.py:310
  103.7 10.5 %all-to-all-done.1 = bf16[32,8,256]{2,1,0:T(8,128)(2,1)S(1)} async-done(((bf16[32,8,256]{2,1,0:T(8,128)(2,1)}), bf16[32,8,256]{2,1,0:T(8,128)(2,1)S(1)}, u32[]{:S(2)}, u32[]{:S(2)}) %all-to-all-start.1) | async-done | bytes 131104 | tf_op jit(solution)/shard_map/all_to_all | solution.py:359
  114.4 34.9 %all_to_all.15 = bf16[8,256,256]{2,1,0:T(8,128)(2,1)S(1)} all-to-all(bf16[8,256,256]{2,1,0:T(8,128)(2,1)S(1)} %shard_map.175), channel_id=1, replica_groups=mesh['grp'=2,'row'=32,'col'=8] {'col'}, dimensions={0} | all-to-all | bytes 2097152 | tf_op jit(solution)/shard_map/all_to_all | solution.py:368
  149.2 1.4 fusion
  (44 shorter events, 7.0 us)
Async XLA Ops:
  0.0 149.2 %copy-start = (bf16[2048,512]{1,0:T(8,128)(2,1)S(1)}, bf16[2048,512]{1,0:T(8,128)(2,1)}, u32[]{:S(2)}) copy-start(bf16[2048,512]{1,0:T(8,128)(2,1)} %param.30) | copy-start | bytes 6291460
  0.0 1.1 copy-start.2
  1.1 0.9 copy-start.3
  2.8 74.0 %all-to-all-start = ((bf16[32,16,256]{2,1,0:T(8,128)(2,1)}), bf16[32,16,256]{2,1,0:T(8,128)(2,1)S(1)}, u32[]{:S(2)}, u32[]{:S(2)}) async-start(bf16[32,16,256]{2,1,0:T(8,128)(2,1)} %shard_map.172), calls=%async_computation | async-start | bytes 524288 | tf_op jit(solution)/shard_map/all_to_all | solution.py:305
  52.0 0.8 copy-start.4
  52.9 0.7 copy-start.5
  53.5 0.7 copy-start.6
  54.2 0.7 copy-start.7
  54.8 1.0 copy-start.8
  55.9 1.0 copy-start.10
  56.9 0.9 copy-start.13
  57.8 0.7 copy-start.15
  58.5 18.3 %copy-start.9 = (bf16[2,512,256]{2,1,0:T(8,128)(2,1)S(1)}, bf16[2,512,256]{2,1,0:T(8,128)(2,1)}, u32[]{:S(2)}) copy-start(bf16[2,512,256]{2,1,0:T(8,128)(2,1)} %constant.26.clone.pair_ref) | copy-start | bytes 1572868
  58.5 18.3 %copy-start.11 = (bf16[2,512,256]{2,1,0:T(8,128)(2,1)S(1)}, bf16[2,512,256]{2,1,0:T(8,128)(2,1)}, u32[]{:S(2)}) copy-start(bf16[2,512,256]{2,1,0:T(8,128)(2,1)} %constant.25.clone.into_ref) | copy-start | bytes 1572868
  75.2 0.8 copy-start.16
  76.0 0.8 copy-start.18
  76.8 1.0 copy-start.12
  77.9 0.9 copy-start.14
  78.8 1.0 copy-start.17
  79.8 1.0 copy-start.19
  80.9 16.8 %copy-start.1 = (bf16[256,256]{1,0:T(8,128)(2,1)S(1)}, bf16[256,256]{1,0:T(8,128)(2,1)}, u32[]{:S(2)}) copy-start(bf16[256,256]{1,0:T(8,128)(2,1)} %gate_ref.1) | copy-start | bytes 393220
  85.2 28.9 %all-to-all-start.1 = ((bf16[32,8,256]{2,1,0:T(8,128)(2,1)}), bf16[32,8,256]{2,1,0:T(8,128)(2,1)S(1)}, u32[]{:S(2)}, u32[]{:S(2)}) async-start(bf16[32,8,256]{2,1,0:T(8,128)(2,1)} %shard_map.174), calls=%async_computation.1 | async-start | bytes 262144 | tf_op jit(solution)/shard_map/all_to_all | solution.py:359
  97.7 3.8 %collective-permute-start = (bf16[1,256]{1,0:T(2,128)(2,1)S(1)}, bf16[1,256]{1,0:T(2,128)(2,1)S(1)}, u32[]{:S(2)}, u32[]{:S(2)}) collective-permute-start(bf16[1,256]{1,0:T(2,128)(2,1)S(1)} %get-tuple-element.9), channel_id=1, source_target_pairs={{0,8},{8,16},{16,24},{24,32},{32,40},{40,48},{48,56},{56,64},{64,7... | collective-permute-start | bytes 1544 | tf_op jit(solution)/shard_map/ppermute | solution.py:310
  99.4 4.2 %collective-permute-start.1 = (bf16[1,256]{1,0:T(2,128)(2,1)S(1)}, bf16[1,256]{1,0:T(2,128)(2,1)S(1)}, u32[]{:S(2)}, u32[]{:S(2)}) collective-permute-start(bf16[1,256]{1,0:T(2,128)(2,1)S(1)} %get-tuple-element.10), channel_id=1, source_target_pairs={{8,0},{16,8},{24,16},{32,24},{40,32},{48,40},{56,48},{64,56},{72,6... | collective-permute-start | bytes 1544 | tf_op jit(solution)/shard_map/ppermute | solution.py:310

commit v2 on v1

--- a/solution.py
+++ b/solution.py
@@ -10,6 +10,7 @@
 from jax.sharding import PartitionSpec as P
 
 ENERGY_FLOOR = 1.0
+UNROLL = 8
 F32 = jnp.float32
 BF16 = jnp.bfloat16
 
@@ -42,7 +43,7 @@
 
 def fit_sine():
     nodes = 0.25 * np.cos(np.pi * (np.arange(64) + 0.5) / 128)
-    powers = np.stack([nodes ** (2 * i + 1) for i in range(5)], 1)
+    powers = np.stack([nodes ** (2 * i + 1) for i in range(4)], 1)
     return [float(v) for v in np.linalg.lstsq(powers, -np.sin(2 * np.pi * nodes), rcond=None)[0]]
 
 
@@ -122,7 +123,7 @@
 
 
 def filter_kernel(
-    rows, chan, embed_ref, first_bias_ref, freq_ref, inner_ref, second_bias_ref, weight_ref, decay_ref,
+    rows, chan, one, embed_ref, first_bias_ref, freq_ref, inner_ref, second_bias_ref, weight_ref, decay_ref,
     band_ref, into_ref, pair_ref, twiddle_ref, spec_re_ref, spec_im_ref,
     first_table, second_table, taps_ref, energy_ref, near_ref, far_ref, first_w, second_w, last_w,
 ):
@@ -130,17 +131,17 @@
     hidden = freq_ref.shape[1]
     seq_len = rows * block
     freq = freq_ref[...] * (0.5 / math.pi)
-    w_one, w_two = halves(embed_ref[...] * freq)
-    first_w[:, :hidden] = jnp.concatenate([w_one, w_one], 0)
-    first_w[:, hidden:] = jnp.concatenate([w_two, w_two], 0)
+    second_bias = second_bias_ref[...] * freq - 0.25
+    spare = lax.broadcasted_iota(jnp.int32, embed_ref.shape, 0) == one
+    first_bias = first_bias_ref[...] * freq - 0.25
+    w_one, w_two = halves(jnp.where(spare, first_bias, embed_ref[...] * freq))
+    first_w[...] = jnp.concatenate([w_one, w_one, w_two, jnp.zeros_like(w_two)], 0)
     v_one, v_two = halves(inner_ref[...] * freq)
     second_w[:, :hidden] = jnp.concatenate([v_one, v_one], 0)
     second_w[:, hidden:] = jnp.concatenate([v_two, v_two], 0)
     u_one, u_two = halves(weight_ref[...])
     last_w[:, :hidden] = jnp.concatenate([u_one, u_two], 0)
     last_w[:, hidden:] = jnp.concatenate([u_one, jnp.zeros_like(u_two)], 0)
-    first_bias = first_bias_ref[...] * freq - 0.25
-    second_bias = second_bias_ref[...] * freq - 0.25
     band = band_ref[0:1]
     shift = band_ref[1:2]
     line = band_ref[2:3]
@@ -162,8 +163,7 @@
     def lags(row):
         feature = first_table[...] * near_ref[pl.ds(row, 1), :] + second_table[...] * far_ref[pl.ds(row, 1), :]
         x_one, x_two = halves(feature)
-        both = dot(jnp.where(left, x_one, x_two), first_w[...])
-        layer_one = cos_turns(both[:, :hidden] + both[:, hidden:] + first_bias)
+        layer_one = cos_turns(dot(jnp.concatenate([jnp.where(left, x_one, x_two), x_one], 1), first_w[...]))
         y_one, y_two = halves(layer_one)
         both = dot(jnp.concatenate([y_one, y_two], 1), second_w[...])
         layer_two = cos_turns(both[:, :hidden] + both[:, hidden:] + second_bias)
@@ -176,12 +176,12 @@
         taps = raw * jnp.exp(decay * (at.astype(F32) * (-1.0 / seq_len)))
         return jnp.where(is_back & (at == 0), 0.0, taps)
 
-    @pl.loop(0, rows // 2)
+    @pl.loop(0, rows // UNROLL)
     def _(step):
-        found = [lags(2 * step + k) for k in range(2)]
-        energy_ref[...] += found[0] * found[0] + found[1] * found[1]
-        for k in range(2):
-            place = pl.multiple_of((2 * step + k) * chan, chan)
+        found = [lags(UNROLL * step + k) for k in range(UNROLL)]
+        energy_ref[...] += sum(taps * taps for taps in found)
+        for k in range(UNROLL):
+            place = pl.multiple_of((UNROLL * step + k) * chan, chan)
             for order in range(parts // (2 * chan)):
                 base = order * 2 * chan
                 ahead = found[k][base : base + chan]
@@ -275,13 +275,13 @@
         out_ref[peer] = gated
 
 
-def call(kernel, out_shape, scratch=(), flops=0, limit=12):
+def call(kernel, out_shape, scratch=(), flops=0, grant=None):
     return pl.pallas_call(
         kernel,
         out_shape=out_shape,
         scratch_shapes=scratch,
         cost_estimate=pl.CostEstimate(flops=flops, bytes_accessed=0, transcendentals=0),
-        compiler_params=pltpu.CompilerParams(vmem_limit_bytes=limit << 20),
+        compiler_params=pltpu.CompilerParams(vmem_limit_bytes=grant),
     )
 
 
@@ -331,7 +331,7 @@
     parts = weight_here.shape[0]
     spec_shape = jax.ShapeDtypeStruct((orders, edge, block), F32)
     spec_re, spec_im = call(
-        functools.partial(filter_kernel, rows, chan),
+        functools.partial(filter_kernel, rows, chan, features),
         (spec_shape, spec_shape),
         (
             pltpu.VMEM((block, 2 * width), F32),
@@ -340,12 +340,11 @@
             pltpu.VMEM((parts, block), F32),
             pltpu.VMEM((rows, 2 * width), F32),
             pltpu.VMEM((rows, 2 * width), F32),
-            pltpu.VMEM((2 * width, 2 * hidden), BF16),
+            pltpu.VMEM((4 * width, hidden), BF16),
             pltpu.VMEM((2 * hidden, 2 * hidden), BF16),
             pltpu.VMEM((2 * parts, 2 * hidden), BF16),
         ),
         flops=12_000_000_000,
-        limit=20,
     )(
         embed, embed_bias[None], sine_freq[None], inner_weight, inner_bias[None], weight_here, decay_here,
         band, into, pair, twiddle,
@@ -354,10 +353,9 @@
         functools.partial(conv_kernel, rows, chan, orders),
         jax.ShapeDtypeStruct((rows, chan, block), BF16),
         flops=5_000_000_000,
-        limit=20,
     )(arrived, param, spec_re, spec_im, into, back, pair, twiddle)
     mixed = lax.all_to_all(mixed, "row", 0, 0, tiled=True).reshape(columns, block)
-    gated = call(gate_kernel, jax.ShapeDtypeStruct((peers, block, columns), BF16), limit=12)(
+    gated = call(gate_kernel, jax.ShapeDtypeStruct((peers, block, columns), BF16), grant=12 << 20)(
         mixed, gate_two, halo, conv_taps[1]
     )
     return finish(gated, out_weight)

time: 152 us -> 142 us (0.934)
  local copies, waits for them, and re-layouts: 18.7 us -> 7.14 us
    unnamed x41 -> x7, local copies, waits for them, and re-layouts: 14.1 us -> 0.79 us
    pallas_call x1, Pallas kernels: 4.38 us -> 6.11 us  [per_device(): call(functools.partial(conv_kernel, rows, chan, orders), jax.ShapeDtypeSt...]
  transfers between devices with their start and end apart: 4 -> 4, of which waited for: 2 -> 2; matrix products, arithmetic and copies ran while one was open for 4% -> 6% of each run, Pallas kernels for 11% -> 11%
where the time goes in v2:
time: 142 us; the launch traced here: 141 us
  starting transfers between devices  59.9 us (42%)
  blocking collectives  34.9 us (25%)
  Pallas kernels  23.6 us (17%)
  waiting for transfers between devices  12.7 us (9%)
  local copies, waits for them, and re-layouts  7.14 us (5%)
  other arithmetic  1.43 us (1%)
    all_to_all x1, starting transfers between devices, per_device(): arrived = lax.all_to_all(turned, 'row', 0, 0, tiled=True)  44.4 us
    all_to_all x1, blocking collectives, finish(): everyone = lax.all_to_all(gated, 'col', 0, 0, tiled=True)  34.9 us
    pallas_call x1, Pallas kernels, per_device(): call(functools.partial(filter_kernel, rows, chan, features), (spec_shape,...  15.3 us
    all_to_all x1, starting transfers between devices, per_device(): lax.all_to_all(mixed, 'row', 0, 0, tiled=True).reshape(columns, block)  12.4 us
    all_to_all x1, waiting for transfers between devices, per_device(): lax.all_to_all(mixed, 'row', 0, 0, tiled=True).reshape(columns, block)  10.5 us
    pallas_call x1, Pallas kernels, per_device(): call(functools.partial(conv_kernel, rows, chan, orders), jax.ShapeDtypeSt...  6.11 us
  transfers between devices with their start and end apart: 4, of which 2 were waited for; matrix products, arithmetic and copies ran while one was open for 6% of the time, Pallas kernels for 11%

profile of v2, /device:TPU:80, one launch (start us, length us, event | category | flops | bytes accessed | tf_op | source)
XLA Modules:
  0.0 141.2 jit_solution(18369492122651804554)
XLA Ops:
  0.0 2.0 %shard_map.172 = bf16[32,16,256]{2,1,0:T(8,128)(2,1)} custom-call(bf16[256,256]{1,0:T(8,128)(2,1)} %first_ref.1, bf16[256,256]{1,0:T(8,128)(2,1)} %second_ref.1), custom_call_target="tpu_custom_call" | custom-call | tf_op jit(solution)/shard_map/pallas_call | solution.py:304
  2.0 44.4 %all-to-all-start = ((bf16[32,16,256]{2,1,0:T(8,128)(2,1)}), bf16[32,16,256]{2,1,0:T(8,128)(2,1)S(1)}, u32[]{:S(2)}, u32[]{:S(2)}) async-start(bf16[32,16,256]{2,1,0:T(8,128)(2,1)} %shard_map.172), calls=%async_computation | async-start | bytes 524288 | tf_op jit(solution)/shard_map/all_to_all | solution.py:305
  46.4 0.8 constant_dynamic-slice_fusion.2
  47.2 0.8 constant_dynamic-slice_fusion
  47.9 0.1 copy.27
  48.0 0.8 dynamic-slice_convert_fusion
  48.8 0.1 copy.24
  48.9 0.7 reshape.27.decay_ref
  49.5 1.3 constant_dynamic-slice_fusion.1
  50.8 0.8 copy.25
  51.6 0.7 maximum_bitcast_fusion.param_ref
  52.2 1.3 pad.4.embed_ref
  53.6 15.3 %shard_map.173 = (f32[2,264,256]{2,1,0:T(8,128)}, f32[2,264,256]{2,1,0:T(8,128)}) custom-call(f32[64,128]{1,0:T(8,128)} %pad.4.embed_ref, f32[1,128]{1,0:T(1,128)} %bitcast.21, f32[1,128]{1,0:T(1,128)} %bitcast.22, f32[128,128]{1,0:T(8,128)} %inner_ref.1, f32[1,128]{1,0:T(1,128)} %bitcast.23, f32[32,128]{1,0:T(8,128)} %bitcast.20, ...), custom_call_target="tpu_custom_call" | custom-call | flops 12000000000 | tf_op jit(solution)/shard_map/pallas_call | solution.py:333
  68.9 0.7 copy-done.2
  69.6 6.1 %shard_map.174 = bf16[32,8,256]{2,1,0:T(8,128)(2,1)} custom-call(bf16[32,16,256]{2,1,0:T(8,128)(2,1)} %copy-done.2, f32[8,11]{1,0:T(8,128)} %maximum_bitcast_fusion.param_ref, f32[2,264,256]{2,1,0:T(8,128)} %get-tuple-element.7.spec_re_ref, f32[2,264,256]{2,1,0:T(8,128)} %get-tuple-element.8.spec_im_ref, bf16[2,512,256]{2,1,0:T(8,128)(2,1)} %constant.25.clone.into_ref, ...), custom_call_target="tpu_custom_call" | custom-call | flops 5000000000 | tf_op jit(solution)/shard_map/pallas_call | solution.py:352
  75.8 12.4 %all-to-all-start.1 = ((bf16[32,8,256]{2,1,0:T(8,128)(2,1)}), bf16[32,8,256]{2,1,0:T(8,128)(2,1)S(1)}, u32[]{:S(2)}, u32[]{:S(2)}) async-start(bf16[32,8,256]{2,1,0:T(8,128)(2,1)} %shard_map.174), calls=%async_computation.1 | async-start | bytes 262144 | tf_op jit(solution)/shard_map/all_to_all | solution.py:357
  88.2 1.7 %collective-permute-start = (bf16[1,256]{1,0:T(2,128)(2,1)S(1)}, bf16[1,256]{1,0:T(2,128)(2,1)S(1)}, u32[]{:S(2)}, u32[]{:S(2)}) collective-permute-start(bf16[1,256]{1,0:T(2,128)(2,1)S(1)} %get-tuple-element.9), channel_id=1, source_target_pairs={{0,8},{8,16},{16,24},{24,32},{32,40},{40,48},{48,56},{56,64},{64,7... | collective-permute-start | bytes 1544 | tf_op jit(solution)/shard_map/ppermute | solution.py:310
  90.0 1.3 collective-permute-start.1
  91.3 0.7 slice_bitcast_fusion.taps_ref
  92.0 2.2 %collective-permute-done.1 = bf16[1,256]{1,0:T(2,128)(2,1)S(1)} collective-permute-done((bf16[1,256]{1,0:T(2,128)(2,1)S(1)}, bf16[1,256]{1,0:T(2,128)(2,1)S(1)}, u32[]{:S(2)}, u32[]{:S(2)}) %collective-permute-start.1) | collective-permute-done | bytes 544 | tf_op jit(solution)/shard_map/ppermute | solution.py:310
  94.2 10.5 %all-to-all-done.1 = bf16[32,8,256]{2,1,0:T(8,128)(2,1)S(1)} async-done(((bf16[32,8,256]{2,1,0:T(8,128)(2,1)}), bf16[32,8,256]{2,1,0:T(8,128)(2,1)S(1)}, u32[]{:S(2)}, u32[]{:S(2)}) %all-to-all-start.1) | async-done | bytes 131104 | tf_op jit(solution)/shard_map/all_to_all | solution.py:357
  104.7 0.2 shard_map.175
  104.9 34.9 %all_to_all.15 = bf16[8,256,256]{2,1,0:T(8,128)(2,1)S(1)} all-to-all(bf16[8,256,256]{2,1,0:T(8,128)(2,1)S(1)} %shard_map.175), channel_id=1, replica_groups=mesh['grp'=2,'row'=32,'col'=8] {'col'}, dimensions={0} | all-to-all | bytes 2097152 | tf_op jit(solution)/shard_map/all_to_all | solution.py:366
  139.7 1.4 fusion
  (10 shorter events, 0.0 us)
Async XLA Ops:
  0.0 139.7 %copy-start = (bf16[2048,512]{1,0:T(8,128)(2,1)S(1)}, bf16[2048,512]{1,0:T(8,128)(2,1)}, u32[]{:S(2)}) copy-start(bf16[2048,512]{1,0:T(8,128)(2,1)} %param.30) | copy-start | bytes 6291460
  2.0 67.0 %all-to-all-start = ((bf16[32,16,256]{2,1,0:T(8,128)(2,1)}), bf16[32,16,256]{2,1,0:T(8,128)(2,1)S(1)}, u32[]{:S(2)}, u32[]{:S(2)}) async-start(bf16[32,16,256]{2,1,0:T(8,128)(2,1)} %shard_map.172), calls=%async_computation | async-start | bytes 524288 | tf_op jit(solution)/shard_map/all_to_all | solution.py:305
  68.9 0.7 copy-start.2
  69.6 18.5 %copy-start.1 = (bf16[256,256]{1,0:T(8,128)(2,1)S(1)}, bf16[256,256]{1,0:T(8,128)(2,1)}, u32[]{:S(2)}) copy-start(bf16[256,256]{1,0:T(8,128)(2,1)} %gate_ref.1) | copy-start | bytes 393220
  75.8 28.9 %all-to-all-start.1 = ((bf16[32,8,256]{2,1,0:T(8,128)(2,1)}), bf16[32,8,256]{2,1,0:T(8,128)(2,1)S(1)}, u32[]{:S(2)}, u32[]{:S(2)}) async-start(bf16[32,8,256]{2,1,0:T(8,128)(2,1)} %shard_map.174), calls=%async_computation.1 | async-start | bytes 262144 | tf_op jit(solution)/shard_map/all_to_all | solution.py:357
  88.2 3.8 %collective-permute-start = (bf16[1,256]{1,0:T(2,128)(2,1)S(1)}, bf16[1,256]{1,0:T(2,128)(2,1)S(1)}, u32[]{:S(2)}, u32[]{:S(2)}) collective-permute-start(bf16[1,256]{1,0:T(2,128)(2,1)S(1)} %get-tuple-element.9), channel_id=1, source_target_pairs={{0,8},{8,16},{16,24},{24,32},{32,40},{40,48},{48,56},{56,64},{64,7... | collective-permute-start | bytes 1544 | tf_op jit(solution)/shard_map/ppermute | solution.py:310
  90.0 4.2 %collective-permute-start.1 = (bf16[1,256]{1,0:T(2,128)(2,1)S(1)}, bf16[1,256]{1,0:T(2,128)(2,1)S(1)}, u32[]{:S(2)}, u32[]{:S(2)}) collective-permute-start(bf16[1,256]{1,0:T(2,128)(2,1)S(1)} %get-tuple-element.10), channel_id=1, source_target_pairs={{8,0},{16,8},{24,16},{32,24},{40,32},{48,40},{56,48},{64,56},{72,6... | collective-permute-start | bytes 1544 | tf_op jit(solution)/shard_map/ppermute | solution.py:310

commit v3 on v2

--- a/solution.py
+++ b/solution.py
@@ -9,8 +9,10 @@
 from jax.experimental.pallas import tpu as pltpu
 from jax.sharding import PartitionSpec as P
 
+
 ENERGY_FLOOR = 1.0
 UNROLL = 8
+GRANT = 60
 F32 = jnp.float32
 BF16 = jnp.bfloat16
 
@@ -18,6 +20,13 @@
 def halves(value):
     high = value.astype(BF16)
     return high, (value - high.astype(F32)).astype(BF16)
+
+
+def thirds(value):
+    high = value.astype(BF16)
+    rest = value - high.astype(F32)
+    middle = rest.astype(BF16)
+    return high, middle, (rest - middle.astype(F32)).astype(BF16)
 
 
 def dot(left, right):
@@ -123,41 +132,73 @@
 
 
 def filter_kernel(
-    rows, chan, one, embed_ref, first_bias_ref, freq_ref, inner_ref, second_bias_ref, weight_ref, decay_ref,
-    band_ref, into_ref, pair_ref, twiddle_ref, spec_re_ref, spec_im_ref,
-    first_table, second_table, taps_ref, energy_ref, near_ref, far_ref, first_w, second_w, last_w,
+    rows, chan, embed_ref, first_bias_ref, freq_ref, inner_ref, second_bias_ref, weight_ref, decay_ref, conv_taps_ref,
+    skip_ref, halo_ref, band_ref, into_ref, pair_ref, twiddle_ref, spec_re_ref, spec_im_ref, param_ref,
+    first_table, second_table, taps_ref, energy_ref, near_ref, far_ref, embed, first_w, second_w, last_w,
+    into, pair, arrivals,
 ):
+    fetches = [
+        pltpu.make_async_copy(source, target, arrivals.at[k])
+        for k, (source, target) in enumerate(((into_ref, into), (pair_ref, pair)))
+    ]
+    for fetch in fetches:
+        fetch.start()
+    del halo_ref
     block = taps_ref.shape[2]
     hidden = freq_ref.shape[1]
     seq_len = rows * block
+    orders = skip_ref.shape[0]
+    parts = 2 * orders * chan
+    width = embed.shape[0]
+    columns = skip_ref.shape[1]
     freq = freq_ref[...] * (0.5 / math.pi)
     second_bias = second_bias_ref[...] * freq - 0.25
-    spare = lax.broadcasted_iota(jnp.int32, embed_ref.shape, 0) == one
-    first_bias = first_bias_ref[...] * freq - 0.25
-    w_one, w_two = halves(jnp.where(spare, first_bias, embed_ref[...] * freq))
+    count = embed_ref.shape[0]
+    embed[...] = jnp.zeros_like(embed)
+    embed[:count, :] = embed_ref[...] * freq
+    embed[count : count + 1, :] = first_bias_ref[...] * freq - 0.25
+    w_one, w_two = halves(embed[...])
     first_w[...] = jnp.concatenate([w_one, w_one, w_two, jnp.zeros_like(w_two)], 0)
     v_one, v_two = halves(inner_ref[...] * freq)
     second_w[:, :hidden] = jnp.concatenate([v_one, v_one], 0)
     second_w[:, hidden:] = jnp.concatenate([v_two, v_two], 0)
-    u_one, u_two = halves(weight_ref[...])
-    last_w[:, :hidden] = jnp.concatenate([u_one, u_two], 0)
-    last_w[:, hidden:] = jnp.concatenate([u_one, jnp.zeros_like(u_two)], 0)
+    place = lax.broadcasted_iota(jnp.int32, (chan, columns), 1) - lax.axis_index("row") * chan
+    chosen = (place == lax.broadcasted_iota(jnp.int32, (chan, columns), 0)).astype(F32).astype(BF16)
+
+    def choose(table):
+        return lax.dot_general(chosen, table, (((1,), (1,)), ((), ())), preferred_element_type=F32)
+
+    def choose_exactly(table):
+        return sum(choose(part) for part in thirds(table))
+
+    for k in range(2 * orders):
+        u_one, u_two = (
+            choose(part).astype(BF16) for part in halves(weight_ref[k // 2, k % 2])
+        )
+        last_w[k * chan : (k + 1) * chan, :] = jnp.concatenate([u_one, u_one], 1)
+        last_w[parts + k * chan : parts + (k + 1) * chan, :] = jnp.concatenate([u_two, jnp.zeros_like(u_two)], 1)
+    decay = []
+    for order in range(orders):
+        here = choose_exactly(decay_ref[order])
+        decay += [here[:, 0:1], here[:, 1:2]]
+    decay = jnp.concatenate(decay, 0)
+    for k in range(conv_taps_ref.shape[0]):
+        param_ref[k, :, 0:3] = choose(conv_taps_ref[k])
+    param_ref[conv_taps_ref.shape[0], :, 0:orders] = choose_exactly(skip_ref[...])
     band = band_ref[0:1]
     shift = band_ref[1:2]
     line = band_ref[2:3]
-    lag = lax.broadcasted_iota(jnp.int32, (block, 2 * embed_ref.shape[0]), 0).astype(F32)
+    lag = lax.broadcasted_iota(jnp.int32, (block, 2 * width), 0).astype(F32)
     turns = lag * band * (1.0 / seq_len)
     first_table[...] = jnp.where(line > 0, 1.0, cos_turns(turns + shift))
     second_table[...] = jnp.where(line > 0, lag * (1.0 / seq_len), cos_turns(turns + (shift + 0.25)))
-    start = lax.broadcasted_iota(jnp.int32, (rows, 2 * embed_ref.shape[0]), 0).astype(F32)
+    start = lax.broadcasted_iota(jnp.int32, (rows, 2 * width), 0).astype(F32)
     turns = start * band * (1.0 / rows)
     near_ref[...] = jnp.where(line > 0, start * (1.0 / rows), cos_turns(turns))
     far_ref[...] = jnp.where(line > 0, 1.0, cos_turns(turns - 0.25))
     energy_ref[...] = jnp.zeros_like(energy_ref)
-    decay = decay_ref[...]
     lanes = lax.broadcasted_iota(jnp.int32, (1, block), 1)
-    left = lax.broadcasted_iota(jnp.int32, (1, 2 * embed_ref.shape[0]), 1) < embed_ref.shape[0]
-    parts = weight_ref.shape[0]
+    left = lax.broadcasted_iota(jnp.int32, (1, 2 * width), 1) < width
     is_back = (lax.broadcasted_iota(jnp.int32, (parts, 1), 0) // chan) % 2 == 1
 
     def lags(row):
@@ -189,23 +230,25 @@
                 taps_ref[2 * order, pl.ds(place, chan), :] = ahead + behind
                 taps_ref[2 * order + 1, pl.ds(place, chan), :] = ahead - behind
 
+    for fetch in fetches:
+        fetch.wait()
     total = jnp.sum(energy_ref[...], axis=1, keepdims=True)
     cos_part, sin_part = spread(twiddle_ref, 0, chan), spread(twiddle_ref, 1, chan)
     for order in range(parts // (2 * chan)):
         base = order * 2 * chan
         scale = lax.rsqrt(total[base : base + chan] + total[base + chan : base + 2 * chan] + ENERGY_FLOOR)
         scale = jnp.broadcast_to(scale[None], (rows + 1, chan, block)).reshape(-1, block)
-        even_re, even_im = first_stage(taps_ref[2 * order], into_ref, chan)
-        odd_re, odd_im = first_stage(taps_ref[2 * order + 1], into_ref, chan)
+        even_re, even_im = first_stage(taps_ref[2 * order], into, chan)
+        odd_re, odd_im = first_stage(taps_ref[2 * order + 1], into, chan)
         spec_re_ref[order] = scale * pair_product(
-            even_re * cos_part + even_im * sin_part, even_im * cos_part - even_re * sin_part, pair_ref
+            even_re * cos_part + even_im * sin_part, even_im * cos_part - even_re * sin_part, pair
         )
         spec_im_ref[order] = scale * pair_product(
-            odd_im * cos_part - odd_re * sin_part, -(odd_re * cos_part + odd_im * sin_part), pair_ref
+            odd_im * cos_part - odd_re * sin_part, -(odd_re * cos_part + odd_im * sin_part), pair
         )
 
 
-def short(signal, taps, first, rows, chan):
+def short(signal, taps, rows, chan):
     block = signal.shape[1]
     lanes = lax.broadcasted_iota(jnp.int32, signal.shape, 1)
     line = lax.broadcasted_iota(jnp.int32, signal.shape, 0)
@@ -218,38 +261,47 @@
     after = jnp.where(lanes == block - 1, crossed, after)
 
     def tap(k):
-        column = taps[:, first + k : first + k + 1]
+        column = taps[:, k : k + 1]
         return jnp.broadcast_to(column[None], (rows, chan, block)).reshape(size, block)
 
     return before * tap(0) + signal * tap(1) + after * tap(2)
 
 
 def conv_kernel(
-    rows, chan, orders, arrived_ref, param_ref, spec_re_ref, spec_im_ref, into_ref, back_ref, pair_ref,
-    twiddle_ref, out_ref,
+    rows, chan, orders, arrived_ref, param_ref, into_ref, twiddle_ref, pair_ref, spec_re_ref, spec_im_ref, back_ref,
+    out_ref, into, twiddle, pair, spec_re, spec_im, back, arrivals,
 ):
+    sources = (into_ref, twiddle_ref, pair_ref, spec_re_ref, spec_im_ref, back_ref)
+    targets = (into, twiddle, pair, spec_re, spec_im, back)
+    fetches = [
+        pltpu.make_async_copy(source, target, arrivals.at[k])
+        for k, (source, target) in enumerate(zip(sources, targets))
+    ]
+    for fetch in fetches:
+        fetch.start()
     block = arrived_ref.shape[2]
     size = rows * chan
-    param = param_ref[...]
 
     def signal(k):
         return arrived_ref[:, k * chan : (k + 1) * chan, :].astype(F32).reshape(size, block)
 
-    cos_part, sin_part = spread(twiddle_ref, 0, chan), spread(twiddle_ref, 1, chan)
-    current = short(signal(0), param, 6, rows, chan)
+    current = short(signal(0), param_ref[orders], rows, chan)
+    for fetch in fetches:
+        fetch.wait()
+    cos_part, sin_part = spread(twiddle, 0, chan), spread(twiddle, 1, chan)
     for order in range(orders):
-        data_re, data_im = forward(current, into_ref, pair_ref, cos_part, sin_part, chan)
-        spec_re, spec_im = spec_re_ref[order], spec_im_ref[order]
+        data_re, data_im = forward(current, into, pair, cos_part, sin_part, chan)
+        own_re, own_im = spec_re[order], spec_im[order]
         long_part = backward(
-            data_re * spec_re - data_im * spec_im,
-            data_re * spec_im + data_im * spec_re,
-            back_ref, pair_ref, cos_part, sin_part, chan,
+            data_re * own_re - data_im * own_im,
+            data_re * own_im + data_im * own_re,
+            back, pair, cos_part, sin_part, chan,
         )
-        column = param[:, 9 + order : 10 + order]
+        column = param_ref[orders + 1, :, order : order + 1]
         skip = jnp.broadcast_to(column[None], (rows, chan, block)).reshape(size, block)
         current = long_part + skip * current
         if order < orders - 1:
-            current = current * short(signal(order + 1), param, 3 * order, rows, chan)
+            current = current * short(signal(order + 1), param_ref[order], rows, chan)
     out_ref[...] = current.astype(BF16).reshape(rows, chan, block)
 
 
@@ -275,10 +327,12 @@
         out_ref[peer] = gated
 
 
-def call(kernel, out_shape, scratch=(), flops=0, grant=None):
+def call(kernel, out_shape, scratch=(), flops=0, grant=None, placed=None):
+    specs = {} if placed is None else {"in_specs": [pl.BlockSpec(memory_space=space) for space in placed]}
     return pl.pallas_call(
         kernel,
         out_shape=out_shape,
+        **specs,
         scratch_shapes=scratch,
         cost_estimate=pl.CostEstimate(flops=flops, bytes_accessed=0, transcendentals=0),
         compiler_params=pltpu.CompilerParams(vmem_limit_bytes=grant),
@@ -290,11 +344,9 @@
     filter_weight, decay_rate, skip_gain, out_weight,
 ):
     rows = lax.axis_size("row")
-    own = lax.axis_index("row")
     block, columns = gate_one.shape
     orders = skip_gain.shape[0]
     chan = columns // rows
-    offset = own * chan
     hidden = sine_freq.shape[0]
     features = embed_weight.shape[0]
     peers = lax.axis_size("col")
@@ -306,19 +358,10 @@
 
     down = [(k, k + 1) for k in range(rows - 1)]
     up = [(k + 1, k) for k in range(rows - 1)]
-    halo = jnp.concatenate(
-        [lax.ppermute(gate_two[-1:], "row", down), lax.ppermute(gate_two[:1], "row", up)], 0
-    )
-
-    weight_here = lax.dynamic_slice_in_dim(filter_weight, offset, chan, 3)
-    weight_here = jnp.transpose(weight_here.reshape(hidden, -1))
-    decay_here = lax.dynamic_slice_in_dim(decay_rate, offset, chan, 2).reshape(-1, 1)
-    taps_here = lax.dynamic_slice_in_dim(conv_taps, offset, chan, 2).astype(F32).reshape(-1, chan)
-    skip_here = lax.dynamic_slice_in_dim(skip_gain, offset, chan, 1)
-    param = jnp.transpose(jnp.concatenate([taps_here, skip_here], 0))
+    halo = [lax.ppermute(gate_two[-1:], "row", down), lax.ppermute(gate_two[:1], "row", up)]
+    halo = jnp.concatenate(halo, 0)
 
     width = 64
-    embed = jnp.pad(embed_weight, ((0, width - features), (0, 0)))
     steps = np.linspace(0.0001, bands - 1, bands).astype(np.float32)
     band = np.zeros((3, width), np.float32)
     band[0, 1:features] = np.concatenate([steps, steps])
@@ -328,11 +371,12 @@
     band = np.concatenate([band, band], 1)
 
     edge = (rows + 1) * chan
-    parts = weight_here.shape[0]
+    parts = 2 * orders * chan
     spec_shape = jax.ShapeDtypeStruct((orders, edge, block), F32)
-    spec_re, spec_im = call(
-        functools.partial(filter_kernel, rows, chan, features),
-        (spec_shape, spec_shape),
+    vmem, anywhere = pltpu.VMEM, pl.ANY
+    spec_re, spec_im, param = call(
+        functools.partial(filter_kernel, rows, chan),
+        (spec_shape, spec_shape, jax.ShapeDtypeStruct((conv_taps.shape[0] + 1, chan, 4), F32)),
         (
             pltpu.VMEM((block, 2 * width), F32),
             pltpu.VMEM((block, 2 * width), F32),
@@ -340,20 +384,29 @@
             pltpu.VMEM((parts, block), F32),
             pltpu.VMEM((rows, 2 * width), F32),
             pltpu.VMEM((rows, 2 * width), F32),
+            pltpu.VMEM((width, hidden), F32),
             pltpu.VMEM((4 * width, hidden), BF16),
             pltpu.VMEM((2 * hidden, 2 * hidden), BF16),
             pltpu.VMEM((2 * parts, 2 * hidden), BF16),
+            pltpu.VMEM(into.shape, BF16),
+            pltpu.VMEM(pair.shape, BF16),
+            pltpu.SemaphoreType.DMA((2,)),
         ),
         flops=12_000_000_000,
+        placed=[vmem] * 11 + [anywhere] * 2 + [vmem],
     )(
-        embed, embed_bias[None], sine_freq[None], inner_weight, inner_bias[None], weight_here, decay_here,
-        band, into, pair, twiddle,
-    )
+        embed_weight, embed_bias[None], sine_freq[None], inner_weight, inner_bias[None],
+        jnp.transpose(filter_weight, (1, 2, 0, 3)), decay_rate, conv_taps, skip_gain, halo, band, into, pair, twiddle,
+    )
+    fetched = (into, twiddle, pair, spec_re, spec_im, back)
     mixed = call(
         functools.partial(conv_kernel, rows, chan, orders),
         jax.ShapeDtypeStruct((rows, chan, block), BF16),
+        [*(pltpu.VMEM(table.shape, table.dtype) for table in fetched), pltpu.SemaphoreType.DMA((len(fetched),))],
         flops=5_000_000_000,
-    )(arrived, param, spec_re, spec_im, into, back, pair, twiddle)
+        grant=GRANT << 20,
+        placed=[vmem] * 2 + [anywhere] * len(fetched),
+    )(arrived, param, *fetched)
     mixed = lax.all_to_all(mixed, "row", 0, 0, tiled=True).reshape(columns, block)
     gated = call(gate_kernel, jax.ShapeDtypeStruct((peers, block, columns), BF16), grant=12 << 20)(
         mixed, gate_two, halo, conv_taps[1]
@@ -362,7 +415,7 @@
 
 
 def finish(gated, out_weight):
-    peers, block, columns = gated.shape
+    peers, _, columns = gated.shape
     everyone = lax.all_to_all(gated, "col", 0, 0, tiled=True)
     weight = out_weight.reshape(peers, columns, -1)
     return jnp.einsum("crk,ckn->rn", everyone, weight, preferred_element_type=F32).astype(BF16)

time: 142 us -> 144 us (1.014)
  waiting for transfers between devices: 12.7 us -> 19.7 us
  local copies, waits for them, and re-layouts: 7.14 us -> 4.23 us
    all_to_all x1, waiting for transfers between devices: 10.5 us -> 15.8 us  [per_device(): lax.all_to_all(mixed, 'row', 0, 0, tiled=True).reshape(columns, block)]
    all_to_all x1, waiting for transfers between devices: 0.01 us -> 3.9 us  [per_device(): arrived = lax.all_to_all(turned, 'row', 0, 0, tiled=True)]
    all_to_all x1, starting transfers between devices: 12.4 us -> 8.54 us  [per_device(): lax.all_to_all(mixed, 'row', 0, 0, tiled=True).reshape(columns, block)]
    dynamic_slice x4 -> x0, local copies, waits for them, and re-layouts: 3.54 us -> none  [the longest x2 2.04 us: per_device(): weight_here = lax.dynamic_slice_in_dim(filter_weight, offset, chan, 3)]
    all_to_all x1, starting transfers between devices: 44.4 us -> 46.9 us  [per_device(): arrived = lax.all_to_all(turned, 'row', 0, 0, tiled=True)]
    ppermute x1, waiting for transfers between devices: 2.22 us -> 0.01 us  [per_device(): lax.ppermute(gate_two[:1], 'row', up)]
    unnamed x7 -> x9, local copies, waits for them, and re-layouts: 0.79 us -> 2.69 us
  transfers between devices with their start and end apart: 4 -> 4, of which waited for: 2 -> 2; matrix products, arithmetic and copies ran while one was open for 6% -> 2% of each run, Pallas kernels for 11% -> 12%
where the time goes in v3:
time: 144 us
  starting transfers between devices  58.6 us (41%)
  blocking collectives  34.9 us (24%)
  Pallas kernels  24.4 us (17%)
  waiting for transfers between devices  19.7 us (14%)
  local copies, waits for them, and re-layouts  4.23 us (3%)
    all_to_all x1, starting transfers between devices, per_device(): arrived = lax.all_to_all(turned, 'row', 0, 0, tiled=True)  46.9 us
    all_to_all x1, blocking collectives, finish(): everyone = lax.all_to_all(gated, 'col', 0, 0, tiled=True)  34.9 us
    all_to_all x1, waiting for transfers between devices, per_device(): lax.all_to_all(mixed, 'row', 0, 0, tiled=True).reshape(columns, block)  15.8 us
    pallas_call x1, Pallas kernels, per_device(): call(functools.partial(filter_kernel, rows, chan), (spec_shape, spec_shap...  15.5 us
    all_to_all x1, starting transfers between devices, per_device(): lax.all_to_all(mixed, 'row', 0, 0, tiled=True).reshape(columns, block)  8.54 us
    pallas_call x1, Pallas kernels, per_device(): call(functools.partial(conv_kernel, rows, chan, orders), jax.ShapeDtypeSt...  6.91 us
    all_to_all x1, waiting for transfers between devices, per_device(): arrived = lax.all_to_all(turned, 'row', 0, 0, tiled=True)  3.9 us
  transfers between devices with their start and end apart: 4, of which 2 were waited for; matrix products, arithmetic and copies ran while one was open for 2% of the time, Pallas kernels for 12%

profile of v3, /device:TPU:80, one launch (start us, length us, event | category | flops | bytes accessed | tf_op | source)
XLA Modules:
  0.0 143.9 jit_solution(3952738791420915235)
XLA Ops:
  0.0 0.0 copy-start
  0.0 0.9 fusion.1
  0.9 1.8 %collective-permute-start = (bf16[1,256]{1,0:T(2,128)(2,1)S(1)}, bf16[1,256]{1,0:T(2,128)(2,1)S(1)}, u32[]{:S(2)}, u32[]{:S(2)}) collective-permute-start(bf16[1,256]{1,0:T(2,128)(2,1)S(1)} %get-tuple-element.11), channel_id=1, source_target_pairs={{0,8},{8,16},{16,24},{24,32},{32,40},{40,48},{48,56},{56,64},{64,7... | collective-permute-start | bytes 1544 | tf_op jit(solution)/shard_map/ppermute | solution.py:361
  2.7 1.3 collective-permute-start.1
  4.0 1.8 %shard_map.172 = bf16[32,16,256]{2,1,0:T(8,128)(2,1)} custom-call(bf16[256,256]{1,0:T(8,128)(2,1)} %first_ref.1, bf16[256,256]{1,0:T(8,128)(2,1)} %second_ref.1), custom_call_target="tpu_custom_call" | custom-call | tf_op jit(solution)/shard_map/pallas_call | solution.py:356
  5.8 46.9 %all-to-all-start = ((bf16[32,16,256]{2,1,0:T(8,128)(2,1)}), bf16[32,16,256]{2,1,0:T(8,128)(2,1)S(1)}, u32[]{:S(2)}, u32[]{:S(2)}) async-start(bf16[32,16,256]{2,1,0:T(8,128)(2,1)} %shard_map.172), calls=%async_computation | async-start | bytes 524288 | tf_op jit(solution)/shard_map/all_to_all | solution.py:357
  52.8 2.0 %copy.21 = f32[128,2,2,256]{3,0,2,1:T(8,128)} copy(f32[128,2,2,256]{3,2,1,0:T(2,128)} %param.27) | data formatting | bytes 1048576 | tf_op args[9]
  54.7 0.0 collective-permute-done
  54.7 0.0 collective-permute-done.1
  54.7 0.6 pad_maximum_fusion.halo_ref
  55.3 15.5 %shard_map.173 = (f32[2,264,256]{2,1,0:T(8,128)}, f32[2,264,256]{2,1,0:T(8,128)}, f32[4,8,4]{2,1,0:T(8,128)}) custom-call(f32[33,128]{1,0:T(8,128)} %embed_ref.1, f32[1,128]{1,0:T(1,128)} %bitcast.19, f32[1,128]{1,0:T(1,128)} %bitcast.20, f32[128,128]{1,0:T(8,128)} %inner_ref.1, f32[1,128]{1,0:T(1,128)} %bitcast.21, f32[2,2,128,256]{3,2,1,0:T(8,128)} %bitcast.18, ...), custom_call_target="tpu_custom_call" | custom-call | flops 12000000000 | tf_op jit(solution)/shard_map/pallas_call | solution.py:377
  70.9 3.9 %all-to-all-done.arrived_ref = bf16[32,16,256]{2,1,0:T(8,128)(2,1)S(1)} async-done(((bf16[32,16,256]{2,1,0:T(8,128)(2,1)}), bf16[32,16,256]{2,1,0:T(8,128)(2,1)S(1)}, u32[]{:S(2)}, u32[]{:S(2)}) %all-to-all-start) | async-done | bytes 262176 | tf_op jit(solution)/shard_map/all_to_all | solution.py:357
  74.8 0.0 copy-start.3
  74.8 0.7 copy-done.3
  75.5 6.9 %shard_map.174 = bf16[32,8,256]{2,1,0:T(8,128)(2,1)} custom-call(bf16[32,16,256]{2,1,0:T(8,128)(2,1)} %copy-done.3, f32[4,8,4]{2,1,0:T(8,128)} %get-tuple-element.8.param_ref, bf16[2,512,256]{2,1,0:T(8,128)(2,1)} %constant.11.clone.into_ref, f32[2,33,256]{2,1,0:T(8,128)} %constant.13.clone.twiddle_ref, bf16[2,512,256]{2,1,0:T(8,128)(2,1)} %constant.12.clone.pair_ref, ...), custom_call_target="tpu_custom_call" | custom-call | flops 5000000000 | tf_op jit(solution)/shard_map/pallas_call | solution.py:402
  82.4 8.5 %all-to-all-start.1 = ((bf16[32,8,256]{2,1,0:T(8,128)(2,1)}), bf16[32,8,256]{2,1,0:T(8,128)(2,1)S(1)}, u32[]{:S(2)}, u32[]{:S(2)}) async-start(bf16[32,8,256]{2,1,0:T(8,128)(2,1)} %shard_map.174), calls=%async_computation.1 | async-start | bytes 262144 | tf_op jit(solution)/shard_map/all_to_all | solution.py:410
  90.9 0.7 slice_bitcast_fusion.taps_ref
  91.6 15.8 %all-to-all-done.1 = bf16[32,8,256]{2,1,0:T(8,128)(2,1)S(1)} async-done(((bf16[32,8,256]{2,1,0:T(8,128)(2,1)}), bf16[32,8,256]{2,1,0:T(8,128)(2,1)S(1)}, u32[]{:S(2)}, u32[]{:S(2)}) %all-to-all-start.1) | async-done | bytes 131104 | tf_op jit(solution)/shard_map/all_to_all | solution.py:410
  107.4 0.0 copy-done.1
  107.4 0.0 copy-done.2
  107.4 0.2 shard_map.175
  107.6 34.9 %all_to_all.15 = bf16[8,256,256]{2,1,0:T(8,128)(2,1)S(1)} all-to-all(bf16[8,256,256]{2,1,0:T(8,128)(2,1)S(1)} %shard_map.175), channel_id=1, replica_groups=mesh['grp'=2,'row'=32,'col'=8] {'col'}, dimensions={0} | all-to-all | bytes 2097152 | tf_op jit(solution)/shard_map/all_to_all | solution.py:419
  142.5 0.0 copy-done
  142.5 1.4 fusion
  (2 shorter events, 0.0 us)
Async XLA Ops:
  0.0 142.5 %copy-start = (bf16[2048,512]{1,0:T(8,128)(2,1)S(1)}, bf16[2048,512]{1,0:T(8,128)(2,1)}, u32[]{:S(2)}) copy-start(bf16[2048,512]{1,0:T(8,128)(2,1)} %param.30) | copy-start | bytes 6291460
  0.9 53.9 %collective-permute-start = (bf16[1,256]{1,0:T(2,128)(2,1)S(1)}, bf16[1,256]{1,0:T(2,128)(2,1)S(1)}, u32[]{:S(2)}, u32[]{:S(2)}) collective-permute-start(bf16[1,256]{1,0:T(2,128)(2,1)S(1)} %get-tuple-element.11), channel_id=1, source_target_pairs={{0,8},{8,16},{16,24},{24,32},{32,40},{40,48},{48,56},{56,64},{64,7... | collective-permute-start | bytes 1544 | tf_op jit(solution)/shard_map/ppermute | solution.py:361
  2.7 52.0 %collective-permute-start.1 = (bf16[1,256]{1,0:T(2,128)(2,1)S(1)}, bf16[1,256]{1,0:T(2,128)(2,1)S(1)}, u32[]{:S(2)}, u32[]{:S(2)}) collective-permute-start(bf16[1,256]{1,0:T(2,128)(2,1)S(1)} %get-tuple-element.12), channel_id=1, source_target_pairs={{8,0},{16,8},{24,16},{32,24},{40,32},{48,40},{56,48},{64,56},{72,6... | collective-permute-start | bytes 1544 | tf_op jit(solution)/shard_map/ppermute | solution.py:361
  5.8 68.9 %all-to-all-start = ((bf16[32,16,256]{2,1,0:T(8,128)(2,1)}), bf16[32,16,256]{2,1,0:T(8,128)(2,1)S(1)}, u32[]{:S(2)}, u32[]{:S(2)}) async-start(bf16[32,16,256]{2,1,0:T(8,128)(2,1)} %shard_map.172), calls=%async_computation | async-start | bytes 524288 | tf_op jit(solution)/shard_map/all_to_all | solution.py:357
  74.8 0.7 copy-start.3
  75.5 32.0 %copy-start.1 = (bf16[256,256]{1,0:T(8,128)(2,1)S(1)}, bf16[256,256]{1,0:T(8,128)(2,1)}, u32[]{:S(2)}) copy-start(bf16[256,256]{1,0:T(8,128)(2,1)} %gate_ref.1) | copy-start | bytes 393220
  75.5 32.0 %copy-start.2 = (bf16[2,256]{1,0:T(2,128)(2,1)S(1)}, bf16[2,256]{1,0:T(2,128)(2,1)}, u32[]{:S(2)}) copy-start(bf16[2,256]{1,0:T(2,128)(2,1)} %pad_maximum_fusion.halo_ref) | copy-start | bytes 3076
  82.4 25.1 %all-to-all-start.1 = ((bf16[32,8,256]{2,1,0:T(8,128)(2,1)}), bf16[32,8,256]{2,1,0:T(8,128)(2,1)S(1)}, u32[]{:S(2)}, u32[]{:S(2)}) async-start(bf16[32,8,256]{2,1,0:T(8,128)(2,1)} %shard_map.174), calls=%async_computation.1 | async-start | bytes 262144 | tf_op jit(solution)/shard_map/all_to_all | solution.py:410

commit v4 on v3

--- a/solution.py
+++ b/solution.py
@@ -9,10 +9,8 @@
 from jax.experimental.pallas import tpu as pltpu
 from jax.sharding import PartitionSpec as P
 
-
 ENERGY_FLOOR = 1.0
 UNROLL = 8
-GRANT = 60
 F32 = jnp.float32
 BF16 = jnp.bfloat16
 
@@ -133,7 +131,7 @@
 
 def filter_kernel(
     rows, chan, embed_ref, first_bias_ref, freq_ref, inner_ref, second_bias_ref, weight_ref, decay_ref, conv_taps_ref,
-    skip_ref, halo_ref, band_ref, into_ref, pair_ref, twiddle_ref, spec_re_ref, spec_im_ref, param_ref,
+    skip_ref, band_ref, into_ref, pair_ref, twiddle_ref, spec_re_ref, spec_im_ref, param_ref,
     first_table, second_table, taps_ref, energy_ref, near_ref, far_ref, embed, first_w, second_w, last_w,
     into, pair, arrivals,
 ):
@@ -143,7 +141,6 @@
     ]
     for fetch in fetches:
         fetch.start()
-    del halo_ref
     block = taps_ref.shape[2]
     hidden = freq_ref.shape[1]
     seq_len = rows * block
@@ -268,34 +265,24 @@
 
 
 def conv_kernel(
-    rows, chan, orders, arrived_ref, param_ref, into_ref, twiddle_ref, pair_ref, spec_re_ref, spec_im_ref, back_ref,
-    out_ref, into, twiddle, pair, spec_re, spec_im, back, arrivals,
+    rows, chan, orders, arrived_ref, param_ref, spec_re_ref, spec_im_ref, into_ref, back_ref, pair_ref,
+    twiddle_ref, out_ref,
 ):
-    sources = (into_ref, twiddle_ref, pair_ref, spec_re_ref, spec_im_ref, back_ref)
-    targets = (into, twiddle, pair, spec_re, spec_im, back)
-    fetches = [
-        pltpu.make_async_copy(source, target, arrivals.at[k])
-        for k, (source, target) in enumerate(zip(sources, targets))
-    ]
-    for fetch in fetches:
-        fetch.start()
     block = arrived_ref.shape[2]
     size = rows * chan
 
     def signal(k):
         return arrived_ref[:, k * chan : (k + 1) * chan, :].astype(F32).reshape(size, block)
 
+    cos_part, sin_part = spread(twiddle_ref, 0, chan), spread(twiddle_ref, 1, chan)
     current = short(signal(0), param_ref[orders], rows, chan)
-    for fetch in fetches:
-        fetch.wait()
-    cos_part, sin_part = spread(twiddle, 0, chan), spread(twiddle, 1, chan)
     for order in range(orders):
-        data_re, data_im = forward(current, into, pair, cos_part, sin_part, chan)
-        own_re, own_im = spec_re[order], spec_im[order]
+        data_re, data_im = forward(current, into_ref, pair_ref, cos_part, sin_part, chan)
+        spec_re, spec_im = spec_re_ref[order], spec_im_ref[order]
         long_part = backward(
-            data_re * own_re - data_im * own_im,
-            data_re * own_im + data_im * own_re,
-            back, pair, cos_part, sin_part, chan,
+            data_re * spec_re - data_im * spec_im,
+            data_re * spec_im + data_im * spec_re,
+            back_ref, pair_ref, cos_part, sin_part, chan,
         )
         column = param_ref[orders + 1, :, order : order + 1]
         skip = jnp.broadcast_to(column[None], (rows, chan, block)).reshape(size, block)
@@ -393,20 +380,16 @@
             pltpu.SemaphoreType.DMA((2,)),
         ),
         flops=12_000_000_000,
-        placed=[vmem] * 11 + [anywhere] * 2 + [vmem],
+        placed=[vmem] * 10 + [anywhere] * 2 + [vmem],
     )(
         embed_weight, embed_bias[None], sine_freq[None], inner_weight, inner_bias[None],
-        jnp.transpose(filter_weight, (1, 2, 0, 3)), decay_rate, conv_taps, skip_gain, halo, band, into, pair, twiddle,
-    )
-    fetched = (into, twiddle, pair, spec_re, spec_im, back)
+        jnp.transpose(filter_weight, (1, 2, 0, 3)), decay_rate, conv_taps, skip_gain, band, into, pair, twiddle,
+    )
     mixed = call(
         functools.partial(conv_kernel, rows, chan, orders),
         jax.ShapeDtypeStruct((rows, chan, block), BF16),
-        [*(pltpu.VMEM(table.shape, table.dtype) for table in fetched), pltpu.SemaphoreType.DMA((len(fetched),))],
         flops=5_000_000_000,
-        grant=GRANT << 20,
-        placed=[vmem] * 2 + [anywhere] * len(fetched),
-    )(arrived, param, *fetched)
+    )(arrived, param, spec_re, spec_im, into, back, pair, twiddle)
     mixed = lax.all_to_all(mixed, "row", 0, 0, tiled=True).reshape(columns, block)
     gated = call(gate_kernel, jax.ShapeDtypeStruct((peers, block, columns), BF16), grant=12 << 20)(
         mixed, gate_two, halo, conv_taps[1]
@@ -415,7 +398,7 @@
 
 
 def finish(gated, out_weight):
-    peers, _, columns = gated.shape
+    peers, block, columns = gated.shape
     everyone = lax.all_to_all(gated, "col", 0, 0, tiled=True)
     weight = out_weight.reshape(peers, columns, -1)
     return jnp.einsum("crk,ckn->rn", everyone, weight, preferred_element_type=F32).astype(BF16)

time: 144 us -> 137 us (0.951)
  starting transfers between devices: 58.6 us -> 55.4 us
  waiting for transfers between devices: 19.7 us -> 17.2 us
    all_to_all x1, waiting for transfers between devices: 15.8 us -> 10.5 us  [per_device(): lax.all_to_all(mixed, 'row', 0, 0, tiled=True).reshape(columns, block)]
    all_to_all x1, starting transfers between devices: 46.9 us -> 44.4 us  [per_device(): arrived = lax.all_to_all(turned, 'row', 0, 0, tiled=True)]
    ppermute x1, waiting for transfers between devices: 0.01 us -> 2.22 us  [per_device(): lax.ppermute(gate_two[:1], 'row', up)]
  transfers between devices with their start and end apart: 4 -> 4, of which waited for: 2 -> 3; matrix products, arithmetic and copies ran while one was open for 2% -> 2% of each run, Pallas kernels for 12% -> 11%
where the time goes in v4:
time: 137 us; the launch traced here: 136 us
  starting transfers between devices  55.4 us (40%)
  blocking collectives  34.9 us (25%)
  Pallas kernels  23.8 us (17%)
  waiting for transfers between devices  17.2 us (13%)
  local copies, waits for them, and re-layouts  3.36 us (2%)
  matrix products  1.41 us (1%)
    all_to_all x1, starting transfers between devices, per_device(): arrived = lax.all_to_all(turned, 'row', 0, 0, tiled=True)  44.4 us
    all_to_all x1, blocking collectives, finish(): everyone = lax.all_to_all(gated, 'col', 0, 0, tiled=True)  34.9 us
    pallas_call x1, Pallas kernels, per_device(): call(functools.partial(filter_kernel, rows, chan), (spec_shape, spec_shap...  15.5 us
    all_to_all x1, waiting for transfers between devices, per_device(): lax.all_to_all(mixed, 'row', 0, 0, tiled=True).reshape(columns, block)  10.5 us
    all_to_all x1, starting transfers between devices, per_device(): lax.all_to_all(mixed, 'row', 0, 0, tiled=True).reshape(columns, block)  7.89 us
    pallas_call x1, Pallas kernels, per_device(): call(functools.partial(conv_kernel, rows, chan, orders), jax.ShapeDtypeSt...  6.14 us
    all_to_all x1, waiting for transfers between devices, per_device(): arrived = lax.all_to_all(turned, 'row', 0, 0, tiled=True)  4.52 us
  transfers between devices with their start and end apart: 4, of which 3 were waited for; matrix products, arithmetic and copies ran while one was open for 2% of the time, Pallas kernels for 11%

profile of v4, /device:TPU:80, one launch (start us, length us, event | category | flops | bytes accessed | tf_op | source)
XLA Modules:
  0.0 136.1 jit_solution(3706036618510232106)
XLA Ops:
  0.0 0.0 copy-start
  0.0 2.0 %shard_map.172 = bf16[32,16,256]{2,1,0:T(8,128)(2,1)} custom-call(bf16[256,256]{1,0:T(8,128)(2,1)} %first_ref.1, bf16[256,256]{1,0:T(8,128)(2,1)} %second_ref.1), custom_call_target="tpu_custom_call" | custom-call | tf_op jit(solution)/shard_map/pallas_call | solution.py:343
  2.0 44.4 %all-to-all-start = ((bf16[32,16,256]{2,1,0:T(8,128)(2,1)}), bf16[32,16,256]{2,1,0:T(8,128)(2,1)S(1)}, u32[]{:S(2)}, u32[]{:S(2)}) async-start(bf16[32,16,256]{2,1,0:T(8,128)(2,1)} %shard_map.172), calls=%async_computation | async-start | bytes 524288 | tf_op jit(solution)/shard_map/all_to_all | solution.py:344
  46.4 2.0 %copy.21 = f32[128,2,2,256]{3,0,2,1:T(8,128)} copy(f32[128,2,2,256]{3,2,1,0:T(2,128)} %param.27) | data formatting | bytes 1048576 | tf_op args[9]
  48.4 15.5 %shard_map.173 = (f32[2,264,256]{2,1,0:T(8,128)}, f32[2,264,256]{2,1,0:T(8,128)}, f32[4,8,4]{2,1,0:T(8,128)}) custom-call(f32[33,128]{1,0:T(8,128)} %embed_ref.1, f32[1,128]{1,0:T(1,128)} %bitcast.19, f32[1,128]{1,0:T(1,128)} %bitcast.20, f32[128,128]{1,0:T(8,128)} %inner_ref.1, f32[1,128]{1,0:T(1,128)} %bitcast.21, f32[2,2,128,256]{3,2,1,0:T(8,128)} %bitcast.18, ...), custom_call_target="tpu_custom_call" | custom-call | flops 12000000000 | tf_op jit(solution)/shard_map/pallas_call | solution.py:364
  63.9 4.5 %all-to-all-done.arrived_ref = bf16[32,16,256]{2,1,0:T(8,128)(2,1)S(1)} async-done(((bf16[32,16,256]{2,1,0:T(8,128)(2,1)}), bf16[32,16,256]{2,1,0:T(8,128)(2,1)S(1)}, u32[]{:S(2)}, u32[]{:S(2)}) %all-to-all-start) | async-done | bytes 262176 | tf_op jit(solution)/shard_map/all_to_all | solution.py:344
  68.4 0.0 copy-start.2
  68.4 0.7 copy-done.2
  69.1 0.0 copy-start.1
  69.1 6.1 %shard_map.174 = bf16[32,8,256]{2,1,0:T(8,128)(2,1)} custom-call(bf16[32,16,256]{2,1,0:T(8,128)(2,1)} %copy-done.2, f32[4,8,4]{2,1,0:T(8,128)} %get-tuple-element.8.param_ref, f32[2,264,256]{2,1,0:T(8,128)} %get-tuple-element.9.spec_re_ref, f32[2,264,256]{2,1,0:T(8,128)} %get-tuple-element.10.spec_im_ref, bf16[2,512,256]{2,1,0:T(8,128)(2,1)} %constant.11.clone.into_ref, ...), custom_call_target="tpu_custom_call" | custom-call | flops 5000000000 | tf_op jit(solution)/shard_map/pallas_call | solution.py:388
  75.3 7.9 %all-to-all-start.1 = ((bf16[32,8,256]{2,1,0:T(8,128)(2,1)}), bf16[32,8,256]{2,1,0:T(8,128)(2,1)S(1)}, u32[]{:S(2)}, u32[]{:S(2)}) async-start(bf16[32,8,256]{2,1,0:T(8,128)(2,1)} %shard_map.174), calls=%async_computation.1 | async-start | bytes 262144 | tf_op jit(solution)/shard_map/all_to_all | solution.py:393
  83.2 0.0 copy-done.1
  83.2 1.7 %collective-permute-start = (bf16[1,256]{1,0:T(2,128)(2,1)S(1)}, bf16[1,256]{1,0:T(2,128)(2,1)S(1)}, u32[]{:S(2)}, u32[]{:S(2)}) collective-permute-start(bf16[1,256]{1,0:T(2,128)(2,1)S(1)} %get-tuple-element.11), channel_id=1, source_target_pairs={{0,8},{8,16},{16,24},{24,32},{32,40},{40,48},{48,56},{56,64},{64,7... | collective-permute-start | bytes 1544 | tf_op jit(solution)/shard_map/ppermute | solution.py:348
  84.9 1.3 collective-permute-start.1
  86.3 0.7 slice_bitcast_fusion.taps_ref
  86.9 0.0 collective-permute-done
  86.9 2.2 %collective-permute-done.1 = bf16[1,256]{1,0:T(2,128)(2,1)S(1)} collective-permute-done((bf16[1,256]{1,0:T(2,128)(2,1)S(1)}, bf16[1,256]{1,0:T(2,128)(2,1)S(1)}, u32[]{:S(2)}, u32[]{:S(2)}) %collective-permute-start.1) | collective-permute-done | bytes 544 | tf_op jit(solution)/shard_map/ppermute | solution.py:348
  89.2 10.5 %all-to-all-done.1 = bf16[32,8,256]{2,1,0:T(8,128)(2,1)S(1)} async-done(((bf16[32,8,256]{2,1,0:T(8,128)(2,1)}), bf16[32,8,256]{2,1,0:T(8,128)(2,1)S(1)}, u32[]{:S(2)}, u32[]{:S(2)}) %all-to-all-start.1) | async-done | bytes 131104 | tf_op jit(solution)/shard_map/all_to_all | solution.py:393
  99.7 0.2 shard_map.175
  99.9 34.9 %all_to_all.15 = bf16[8,256,256]{2,1,0:T(8,128)(2,1)S(1)} all-to-all(bf16[8,256,256]{2,1,0:T(8,128)(2,1)S(1)} %shard_map.175), channel_id=1, replica_groups=mesh['grp'=2,'row'=32,'col'=8] {'col'}, dimensions={0} | all-to-all | bytes 2097152 | tf_op jit(solution)/shard_map/all_to_all | solution.py:402
  134.7 0.0 copy-done
  134.7 1.4 %fusion = bf16[256,512]{1,0:T(8,128)(2,1)} fusion(bf16[8,256,256]{2,1,0:T(8,128)(2,1)S(1)} %all_to_all.15, bf16[8,256,512]{2,1,0:T(8,128)(2,1)S(1)} %bitcast.16), kind=kOutput, calls=%fused_computation.1 | convolution fusion | flops 537001984 | bytes 3407872 | tf_op jit(solution)/shard_map/crk,ckn->rn/dot_general | solution.py:404
  (2 shorter events, 0.0 us)
Async XLA Ops:
  0.0 134.7 %copy-start = (bf16[2048,512]{1,0:T(8,128)(2,1)S(1)}, bf16[2048,512]{1,0:T(8,128)(2,1)}, u32[]{:S(2)}) copy-start(bf16[2048,512]{1,0:T(8,128)(2,1)} %param.30) | copy-start | bytes 6291460
  2.0 66.5 %all-to-all-start = ((bf16[32,16,256]{2,1,0:T(8,128)(2,1)}), bf16[32,16,256]{2,1,0:T(8,128)(2,1)S(1)}, u32[]{:S(2)}, u32[]{:S(2)}) async-start(bf16[32,16,256]{2,1,0:T(8,128)(2,1)} %shard_map.172), calls=%async_computation | async-start | bytes 524288 | tf_op jit(solution)/shard_map/all_to_all | solution.py:344
  68.4 0.7 copy-start.2
  69.1 14.0 %copy-start.1 = (bf16[256,256]{1,0:T(8,128)(2,1)S(1)}, bf16[256,256]{1,0:T(8,128)(2,1)}, u32[]{:S(2)}) copy-start(bf16[256,256]{1,0:T(8,128)(2,1)} %gate_ref.1) | copy-start | bytes 393220
  75.3 24.4 %all-to-all-start.1 = ((bf16[32,8,256]{2,1,0:T(8,128)(2,1)}), bf16[32,8,256]{2,1,0:T(8,128)(2,1)S(1)}, u32[]{:S(2)}, u32[]{:S(2)}) async-start(bf16[32,8,256]{2,1,0:T(8,128)(2,1)} %shard_map.174), calls=%async_computation.1 | async-start | bytes 262144 | tf_op jit(solution)/shard_map/all_to_all | solution.py:393
  83.2 3.8 %collective-permute-start = (bf16[1,256]{1,0:T(2,128)(2,1)S(1)}, bf16[1,256]{1,0:T(2,128)(2,1)S(1)}, u32[]{:S(2)}, u32[]{:S(2)}) collective-permute-start(bf16[1,256]{1,0:T(2,128)(2,1)S(1)} %get-tuple-element.11), channel_id=1, source_target_pairs={{0,8},{8,16},{16,24},{24,32},{32,40},{40,48},{48,56},{56,64},{64,7... | collective-permute-start | bytes 1544 | tf_op jit(solution)/shard_map/ppermute | solution.py:348
  84.9 4.2 %collective-permute-start.1 = (bf16[1,256]{1,0:T(2,128)(2,1)S(1)}, bf16[1,256]{1,0:T(2,128)(2,1)S(1)}, u32[]{:S(2)}, u32[]{:S(2)}) collective-permute-start(bf16[1,256]{1,0:T(2,128)(2,1)S(1)} %get-tuple-element.12), channel_id=1, source_target_pairs={{8,0},{16,8},{24,16},{32,24},{40,32},{48,40},{56,48},{64,56},{72,6... | collective-permute-start | bytes 1544 | tf_op jit(solution)/shard_map/ppermute | solution.py:348

commit v5 on v4

--- a/solution.py
+++ b/solution.py
@@ -309,9 +309,7 @@
     before = jnp.where(line == 0, halo[0:1], pltpu.roll(gate, 1, 0))
     after = jnp.where(line == block - 1, halo[1:2], pltpu.roll(gate, block - 1, 0))
     factor = before * taps[0:1] + gate * taps[1:2] + after * taps[2:3]
-    gated = (jnp.transpose(mixed_ref[...].astype(F32)) * factor).astype(BF16)
-    for peer in range(out_ref.shape[0]):
-        out_ref[peer] = gated
+    out_ref[...] = (jnp.transpose(mixed_ref[...].astype(F32)) * factor).astype(BF16)
 
 
 def call(kernel, out_shape, scratch=(), flops=0, grant=None, placed=None):
@@ -336,7 +334,6 @@
     chan = columns // rows
     hidden = sine_freq.shape[0]
     features = embed_weight.shape[0]
-    peers = lax.axis_size("col")
     bands = (features - 1) // 2
     into, back, pair, twiddle = tables(rows, chan, block)
 
@@ -391,17 +388,46 @@
         flops=5_000_000_000,
     )(arrived, param, spec_re, spec_im, into, back, pair, twiddle)
     mixed = lax.all_to_all(mixed, "row", 0, 0, tiled=True).reshape(columns, block)
-    gated = call(gate_kernel, jax.ShapeDtypeStruct((peers, block, columns), BF16), grant=12 << 20)(
+    gated = call(gate_kernel, jax.ShapeDtypeStruct((block, columns), BF16), grant=12 << 20)(
         mixed, gate_two, halo, conv_taps[1]
     )
     return finish(gated, out_weight)
 
 
+def product_kernel(shifts, weight_ref, *refs):
+    out_ref = refs[-1]
+    peers = weight_ref.shape[0]
+    me = lax.axis_index("col")
+    half = out_ref.shape[0] // 2
+    for part in range(2):
+        place = slice(part * half, (part + 1) * half)
+        total = None
+        for shift, ref in zip(shifts, refs):
+            term = dot(ref[place, :], weight_ref[lax.rem(me + (peers - shift), peers)])
+            total = term if total is None else total + term
+        out_ref[place, :] = total.astype(BF16)
+
+
 def finish(gated, out_weight):
-    peers, block, columns = gated.shape
-    everyone = lax.all_to_all(gated, "col", 0, 0, tiled=True)
+    peers = lax.axis_size("col")
+    columns = gated.shape[1]
+
+    def shifted(block, shift):
+        return lax.ppermute(block, "col", [(k, (k + shift) % peers) for k in range(peers)])
+
+    blocks = {0: gated}
+    for shift in (2, peers - 2, 1, peers - 1):
+        blocks[shift] = shifted(gated, shift)
+    blocks[4] = shifted(blocks[2], 2)
+    blocks[3] = shifted(blocks[2], 1)
+    blocks[peers - 3] = shifted(blocks[peers - 2], peers - 1)
     weight = out_weight.reshape(peers, columns, -1)
-    return jnp.einsum("crk,ckn->rn", everyone, weight, preferred_element_type=F32).astype(BF16)
+    return call(
+        functools.partial(product_kernel, tuple(blocks)),
+        jax.ShapeDtypeStruct((gated.shape[0], weight.shape[2]), BF16),
+        flops=1_000_000_000,
+        grant=12 << 20,
+    )(weight, *blocks.values())
 
 
 def solution(mesh):

time: 137 us -> 133 us (0.971)
  blocking collectives: 34.9 us -> 0 us
  starting transfers between devices: 55.4 us -> 80.9 us
  waiting for transfers between devices: 17.2 us -> 22.8 us
  matrix products: 1.41 us -> 0 us
    all_to_all x1 -> x0, blocking collectives: 34.9 us -> none  [finish(): everyone = lax.all_to_all(gated, 'col', 0, 0, tiled=True)]
    ppermute x0 -> x7, starting transfers between devices: none -> 25.4 us  [shifted(): lax.ppermute(block, 'col', [(k, (k + shift) % peers) for k in range(peers)])]
    ppermute x0 -> x7, waiting for transfers between devices: none -> 5.58 us  [shifted(): lax.ppermute(block, 'col', [(k, (k + shift) % peers) for k in range(peers)])]
    dot_general x1 -> x0, matrix products: 1.41 us -> none  [finish(): jnp.einsum('crk,ckn->rn', everyone, weight, preferred_element_type=F32)]
    pallas_call x1 -> x2, Pallas kernels: 0.18 us -> 1.55 us  [the longest x1 1.42 us: finish(): call(functools.partial(product_kernel, tuple(blocks)), jax.ShapeDtypeStru...]
  transfers between devices with their start and end apart: 4 -> 11, of which waited for: 3 -> 6; matrix products, arithmetic and copies ran while one was open for 2% -> 2% of each run, Pallas kernels for 11% -> 12%
where the time goes in v5:
time: 133 us; the launch traced here: 132 us
  starting transfers between devices  80.9 us (61%)
  Pallas kernels  25.1 us (19%)
  waiting for transfers between devices  22.8 us (17%)
  local copies, waits for them, and re-layouts  3.37 us (3%)
    all_to_all x1, starting transfers between devices, per_device(): arrived = lax.all_to_all(turned, 'row', 0, 0, tiled=True)  44.4 us
    ppermute x7, starting transfers between devices, shifted(): lax.ppermute(block, 'col', [(k, (k + shift) % peers) for k in range(peers)])  25.4 us
    pallas_call x1, Pallas kernels, per_device(): call(functools.partial(filter_kernel, rows, chan), (spec_shape, spec_shap...  15.5 us
    all_to_all x1, waiting for transfers between devices, per_device(): lax.all_to_all(mixed, 'row', 0, 0, tiled=True).reshape(columns, block)  10.5 us
    all_to_all x1, starting transfers between devices, per_device(): lax.all_to_all(mixed, 'row', 0, 0, tiled=True).reshape(columns, block)  7.93 us
    pallas_call x1, Pallas kernels, per_device(): call(functools.partial(conv_kernel, rows, chan, orders), jax.ShapeDtypeSt...  6.26 us
    ppermute x7, waiting for transfers between devices, shifted(): lax.ppermute(block, 'col', [(k, (k + shift) % peers) for k in range(peers)])  5.58 us
    all_to_all x1, waiting for transfers between devices, per_device(): arrived = lax.all_to_all(turned, 'row', 0, 0, tiled=True)  4.5 us
  transfers between devices with their start and end apart: 11, of which 6 were waited for; matrix products, arithmetic and copies ran while one was open for 2% of the time, Pallas kernels for 12%

profile of v5, /device:TPU:80, one launch (start us, length us, event | category | flops | bytes accessed | tf_op | source)
XLA Modules:
  0.0 132.3 jit_solution(8364497134235743341)
XLA Ops:
  0.0 1.8 %shard_map.172 = bf16[32,16,256]{2,1,0:T(8,128)(2,1)} custom-call(bf16[256,256]{1,0:T(8,128)(2,1)} %first_ref.1, bf16[256,256]{1,0:T(8,128)(2,1)} %second_ref.1), custom_call_target="tpu_custom_call" | custom-call | tf_op jit(solution)/shard_map/pallas_call | solution.py:340
  1.8 44.4 %all-to-all-start = ((bf16[32,16,256]{2,1,0:T(8,128)(2,1)}), bf16[32,16,256]{2,1,0:T(8,128)(2,1)S(1)}, u32[]{:S(2)}, u32[]{:S(2)}) async-start(bf16[32,16,256]{2,1,0:T(8,128)(2,1)} %shard_map.172), calls=%async_computation | async-start | bytes 524288 | tf_op jit(solution)/shard_map/all_to_all | solution.py:341
  46.3 2.0 %copy.21 = f32[128,2,2,256]{3,0,2,1:T(8,128)} copy(f32[128,2,2,256]{3,2,1,0:T(2,128)} %param.27) | data formatting | bytes 1048576 | tf_op args[9]
  48.2 15.5 %shard_map.173 = (f32[2,264,256]{2,1,0:T(8,128)}, f32[2,264,256]{2,1,0:T(8,128)}, f32[4,8,4]{2,1,0:T(8,128)}) custom-call(f32[33,128]{1,0:T(8,128)} %embed_ref.1, f32[1,128]{1,0:T(1,128)} %bitcast.13, f32[1,128]{1,0:T(1,128)} %bitcast.14, f32[128,128]{1,0:T(8,128)} %inner_ref.1, f32[1,128]{1,0:T(1,128)} %bitcast.15, f32[2,2,128,256]{3,2,1,0:T(8,128)} %bitcast.12, ...), custom_call_target="tpu_custom_call" | custom-call | flops 12000000000 | tf_op jit(solution)/shard_map/pallas_call | solution.py:361
  63.8 4.5 %all-to-all-done.arrived_ref = bf16[32,16,256]{2,1,0:T(8,128)(2,1)S(1)} async-done(((bf16[32,16,256]{2,1,0:T(8,128)(2,1)}), bf16[32,16,256]{2,1,0:T(8,128)(2,1)S(1)}, u32[]{:S(2)}, u32[]{:S(2)}) %all-to-all-start) | async-done | bytes 262176 | tf_op jit(solution)/shard_map/all_to_all | solution.py:341
  68.3 0.7 copy-done.2
  69.0 6.3 %shard_map.174 = bf16[32,8,256]{2,1,0:T(8,128)(2,1)} custom-call(bf16[32,16,256]{2,1,0:T(8,128)(2,1)} %copy-done.2, f32[4,8,4]{2,1,0:T(8,128)} %get-tuple-element.8.param_ref, f32[2,264,256]{2,1,0:T(8,128)} %get-tuple-element.9.spec_re_ref, f32[2,264,256]{2,1,0:T(8,128)} %get-tuple-element.10.spec_im_ref, bf16[2,512,256]{2,1,0:T(8,128)(2,1)} %constant.11.clone.into_ref, ...), custom_call_target="tpu_custom_call" | custom-call | flops 5000000000 | tf_op jit(solution)/shard_map/pallas_call | solution.py:385
  75.2 7.9 %all-to-all-start.1 = ((bf16[32,8,256]{2,1,0:T(8,128)(2,1)}), bf16[32,8,256]{2,1,0:T(8,128)(2,1)S(1)}, u32[]{:S(2)}, u32[]{:S(2)}) async-start(bf16[32,8,256]{2,1,0:T(8,128)(2,1)} %shard_map.174), calls=%async_computation.1 | async-start | bytes 262144 | tf_op jit(solution)/shard_map/all_to_all | solution.py:390
  83.2 1.7 %collective-permute-start = (bf16[1,256]{1,0:T(2,128)(2,1)S(1)}, bf16[1,256]{1,0:T(2,128)(2,1)S(1)}, u32[]{:S(2)}, u32[]{:S(2)}) collective-permute-start(bf16[1,256]{1,0:T(2,128)(2,1)S(1)} %get-tuple-element.11), channel_id=1, source_target_pairs={{0,8},{8,16},{16,24},{24,32},{32,40},{40,48},{48,56},{56,64},{64,7... | collective-permute-start | bytes 1544 | tf_op jit(solution)/shard_map/ppermute | solution.py:345
  84.9 1.3 collective-permute-start.1
  86.3 0.7 slice_bitcast_fusion.taps_ref
  87.0 2.2 %collective-permute-done.1 = bf16[1,256]{1,0:T(2,128)(2,1)S(1)} collective-permute-done((bf16[1,256]{1,0:T(2,128)(2,1)S(1)}, bf16[1,256]{1,0:T(2,128)(2,1)S(1)}, u32[]{:S(2)}, u32[]{:S(2)}) %collective-permute-start.1) | collective-permute-done | bytes 544 | tf_op jit(solution)/shard_map/ppermute | solution.py:345
  89.2 10.5 %all-to-all-done.1 = bf16[32,8,256]{2,1,0:T(8,128)(2,1)S(1)} async-done(((bf16[32,8,256]{2,1,0:T(8,128)(2,1)}), bf16[32,8,256]{2,1,0:T(8,128)(2,1)S(1)}, u32[]{:S(2)}, u32[]{:S(2)}) %all-to-all-start.1) | async-done | bytes 131104 | tf_op jit(solution)/shard_map/all_to_all | solution.py:390
  99.8 4.6 %collective-permute-start.2 = (bf16[256,256]{1,0:T(8,128)(2,1)S(1)}, bf16[256,256]{1,0:T(8,128)(2,1)S(1)}, u32[]{:S(2)}, u32[]{:S(2)}) collective-permute-start(bf16[256,256]{1,0:T(8,128)(2,1)S(1)} %shard_map.175.refs_0_), channel_id=1, source_target_pairs={{0,2},{1,3},{2,4},{3,5},{4,6},{5,7},{6,0},{7,1},{8,10},{9,11},{10,... | collective-permute-start | bytes 393224 | tf_op jit(solution)/shard_map/ppermute | solution.py:416
  104.4 3.8 %collective-permute-start.3 = (bf16[256,256]{1,0:T(8,128)(2,1)S(1)}, bf16[256,256]{1,0:T(8,128)(2,1)S(1)}, u32[]{:S(2)}, u32[]{:S(2)}) collective-permute-start(bf16[256,256]{1,0:T(8,128)(2,1)S(1)} %shard_map.175.refs_0_), channel_id=1, source_target_pairs={{0,6},{1,7},{2,0},{3,1},{4,2},{5,3},{6,4},{7,5},{8,14},{9,15},{10,... | collective-permute-start | bytes 393224 | tf_op jit(solution)/shard_map/ppermute | solution.py:416
  108.3 3.1 %collective-permute-start.4 = (bf16[256,256]{1,0:T(8,128)(2,1)S(1)}, bf16[256,256]{1,0:T(8,128)(2,1)S(1)}, u32[]{:S(2)}, u32[]{:S(2)}) collective-permute-start(bf16[256,256]{1,0:T(8,128)(2,1)S(1)} %shard_map.175.refs_0_), channel_id=1, source_target_pairs={{0,1},{1,2},{2,3},{3,4},{4,5},{5,6},{6,7},{7,0},{8,9},{9,10},{10,1... | collective-permute-start | bytes 393224 | tf_op jit(solution)/shard_map/ppermute | solution.py:416
  111.4 4.0 %collective-permute-start.5 = (bf16[256,256]{1,0:T(8,128)(2,1)S(1)}, bf16[256,256]{1,0:T(8,128)(2,1)S(1)}, u32[]{:S(2)}, u32[]{:S(2)}) collective-permute-start(bf16[256,256]{1,0:T(8,128)(2,1)S(1)} %shard_map.175.refs_0_), channel_id=1, source_target_pairs={{0,7},{1,0},{2,1},{3,2},{4,3},{5,4},{6,5},{7,6},{8,15},{9,8},{10,9... | collective-permute-start | bytes 393224 | tf_op jit(solution)/shard_map/ppermute | solution.py:416
  115.4 2.8 %collective-permute-start.6 = (bf16[256,256]{1,0:T(8,128)(2,1)S(1)}, bf16[256,256]{1,0:T(8,128)(2,1)S(1)}, u32[]{:S(2)}, u32[]{:S(2)}) collective-permute-start(bf16[256,256]{1,0:T(8,128)(2,1)S(1)} %collective-permute-done.2.refs_1_), channel_id=1, source_target_pairs={{0,2},{1,3},{2,4},{3,5},{4,6},{5,7},{6,0},{7,1},{8,10},{9,11},{10,... | collective-permute-start | bytes 393224 | tf_op jit(solution)/shard_map/ppermute | solution.py:416
  118.2 4.6 %collective-permute-start.7 = (bf16[256,256]{1,0:T(8,128)(2,1)S(1)}, bf16[256,256]{1,0:T(8,128)(2,1)S(1)}, u32[]{:S(2)}, u32[]{:S(2)}) collective-permute-start(bf16[256,256]{1,0:T(8,128)(2,1)S(1)} %collective-permute-done.2.refs_1_), channel_id=1, source_target_pairs={{0,1},{1,2},{2,3},{3,4},{4,5},{5,6},{6,7},{7,0},{8,9},{9,10},{10,1... | collective-permute-start | bytes 393224 | tf_op jit(solution)/shard_map/ppermute | solution.py:416
  122.8 2.5 %collective-permute-start.8 = (bf16[256,256]{1,0:T(8,128)(2,1)S(1)}, bf16[256,256]{1,0:T(8,128)(2,1)S(1)}, u32[]{:S(2)}, u32[]{:S(2)}) collective-permute-start(bf16[256,256]{1,0:T(8,128)(2,1)S(1)} %collective-permute-done.3.refs_2_), channel_id=1, source_target_pairs={{0,7},{1,0},{2,1},{3,2},{4,3},{5,4},{6,5},{7,6},{8,15},{9,8},{10,9... | collective-permute-start | bytes 393224 | tf_op jit(solution)/shard_map/ppermute | solution.py:416
  125.3 1.3 collective-permute-done.6.refs_5_
  126.6 1.4 %collective-permute-done.7.refs_6_ = bf16[256,256]{1,0:T(8,128)(2,1)S(1)} collective-permute-done((bf16[256,256]{1,0:T(8,128)(2,1)S(1)}, bf16[256,256]{1,0:T(8,128)(2,1)S(1)}, u32[]{:S(2)}, u32[]{:S(2)}) %collective-permute-start.7) | collective-permute-done | bytes 131104 | tf_op jit(solution)/shard_map/ppermute | solution.py:416
  128.0 2.9 %collective-permute-done.8.refs_7_ = bf16[256,256]{1,0:T(8,128)(2,1)S(1)} collective-permute-done((bf16[256,256]{1,0:T(8,128)(2,1)S(1)}, bf16[256,256]{1,0:T(8,128)(2,1)S(1)}, u32[]{:S(2)}, u32[]{:S(2)}) %collective-permute-start.8) | collective-permute-done | bytes 131104 | tf_op jit(solution)/shard_map/ppermute | solution.py:416
  130.9 1.4 %shard_map.176 = bf16[256,512]{1,0:T(8,128)(2,1)} custom-call(bf16[8,256,512]{2,1,0:T(8,128)(2,1)S(1)} %bitcast.11, bf16[256,256]{1,0:T(8,128)(2,1)S(1)} %shard_map.175.refs_0_, bf16[256,256]{1,0:T(8,128)(2,1)S(1)} %collective-permute-done.2.refs_1_, bf16[256,256]{1,0:T(8,128)(2,1)S(1)} %collective-permute-done.3.refs_2_, ...), custom_call_target="tpu_custom_call" | custom-call | flops 1000000000 | tf_op jit(solution)/shard_map/pallas_call | solution.py:425
  (13 shorter events, 0.2 us)
Async XLA Ops:
  1.8 66.5 %all-to-all-start = ((bf16[32,16,256]{2,1,0:T(8,128)(2,1)}), bf16[32,16,256]{2,1,0:T(8,128)(2,1)S(1)}, u32[]{:S(2)}, u32[]{:S(2)}) async-start(bf16[32,16,256]{2,1,0:T(8,128)(2,1)} %shard_map.172), calls=%async_computation | async-start | bytes 524288 | tf_op jit(solution)/shard_map/all_to_all | solution.py:341
  68.3 0.7 copy-start.2
  69.0 14.2 %copy-start = (bf16[256,256]{1,0:T(8,128)(2,1)S(1)}, bf16[256,256]{1,0:T(8,128)(2,1)}, u32[]{:S(2)}) copy-start(bf16[256,256]{1,0:T(8,128)(2,1)} %gate_ref.1) | copy-start | bytes 393220
  69.0 62.0 %copy-start.1 = (bf16[2048,512]{1,0:T(8,128)(2,1)S(1)}, bf16[2048,512]{1,0:T(8,128)(2,1)}, u32[]{:S(2)}) copy-start(bf16[2048,512]{1,0:T(8,128)(2,1)} %param.30) | copy-start | bytes 6291460
  75.2 24.5 %all-to-all-start.1 = ((bf16[32,8,256]{2,1,0:T(8,128)(2,1)}), bf16[32,8,256]{2,1,0:T(8,128)(2,1)S(1)}, u32[]{:S(2)}, u32[]{:S(2)}) async-start(bf16[32,8,256]{2,1,0:T(8,128)(2,1)} %shard_map.174), calls=%async_computation.1 | async-start | bytes 262144 | tf_op jit(solution)/shard_map/all_to_all | solution.py:390
  83.2 3.8 %collective-permute-start = (bf16[1,256]{1,0:T(2,128)(2,1)S(1)}, bf16[1,256]{1,0:T(2,128)(2,1)S(1)}, u32[]{:S(2)}, u32[]{:S(2)}) collective-permute-start(bf16[1,256]{1,0:T(2,128)(2,1)S(1)} %get-tuple-element.11), channel_id=1, source_target_pairs={{0,8},{8,16},{16,24},{24,32},{32,40},{40,48},{48,56},{56,64},{64,7... | collective-permute-start | bytes 1544 | tf_op jit(solution)/shard_map/ppermute | solution.py:345
  84.9 4.2 %collective-permute-start.1 = (bf16[1,256]{1,0:T(2,128)(2,1)S(1)}, bf16[1,256]{1,0:T(2,128)(2,1)S(1)}, u32[]{:S(2)}, u32[]{:S(2)}) collective-permute-start(bf16[1,256]{1,0:T(2,128)(2,1)S(1)} %get-tuple-element.12), channel_id=1, source_target_pairs={{8,0},{16,8},{24,16},{32,24},{40,32},{48,40},{56,48},{64,56},{72,6... | collective-permute-start | bytes 1544 | tf_op jit(solution)/shard_map/ppermute | solution.py:345
  99.8 15.6 %collective-permute-start.2 = (bf16[256,256]{1,0:T(8,128)(2,1)S(1)}, bf16[256,256]{1,0:T(8,128)(2,1)S(1)}, u32[]{:S(2)}, u32[]{:S(2)}) collective-permute-start(bf16[256,256]{1,0:T(8,128)(2,1)S(1)} %shard_map.175.refs_0_), channel_id=1, source_target_pairs={{0,2},{1,3},{2,4},{3,5},{4,6},{5,7},{6,0},{7,1},{8,10},{9,11},{10,... | collective-permute-start | bytes 393224 | tf_op jit(solution)/shard_map/ppermute | solution.py:416
  104.4 18.4 %collective-permute-start.3 = (bf16[256,256]{1,0:T(8,128)(2,1)S(1)}, bf16[256,256]{1,0:T(8,128)(2,1)S(1)}, u32[]{:S(2)}, u32[]{:S(2)}) collective-permute-start(bf16[256,256]{1,0:T(8,128)(2,1)S(1)} %shard_map.175.refs_0_), channel_id=1, source_target_pairs={{0,6},{1,7},{2,0},{3,1},{4,2},{5,3},{6,4},{7,5},{8,14},{9,15},{10,... | collective-permute-start | bytes 393224 | tf_op jit(solution)/shard_map/ppermute | solution.py:416
  108.3 17.1 %collective-permute-start.4 = (bf16[256,256]{1,0:T(8,128)(2,1)S(1)}, bf16[256,256]{1,0:T(8,128)(2,1)S(1)}, u32[]{:S(2)}, u32[]{:S(2)}) collective-permute-start(bf16[256,256]{1,0:T(8,128)(2,1)S(1)} %shard_map.175.refs_0_), channel_id=1, source_target_pairs={{0,1},{1,2},{2,3},{3,4},{4,5},{5,6},{6,7},{7,0},{8,9},{9,10},{10,1... | collective-permute-start | bytes 393224 | tf_op jit(solution)/shard_map/ppermute | solution.py:416
  111.4 13.9 %collective-permute-start.5 = (bf16[256,256]{1,0:T(8,128)(2,1)S(1)}, bf16[256,256]{1,0:T(8,128)(2,1)S(1)}, u32[]{:S(2)}, u32[]{:S(2)}) collective-permute-start(bf16[256,256]{1,0:T(8,128)(2,1)S(1)} %shard_map.175.refs_0_), channel_id=1, source_target_pairs={{0,7},{1,0},{2,1},{3,2},{4,3},{5,4},{6,5},{7,6},{8,15},{9,8},{10,9... | collective-permute-start | bytes 393224 | tf_op jit(solution)/shard_map/ppermute | solution.py:416
  115.4 11.2 %collective-permute-start.6 = (bf16[256,256]{1,0:T(8,128)(2,1)S(1)}, bf16[256,256]{1,0:T(8,128)(2,1)S(1)}, u32[]{:S(2)}, u32[]{:S(2)}) collective-permute-start(bf16[256,256]{1,0:T(8,128)(2,1)S(1)} %collective-permute-done.2.refs_1_), channel_id=1, source_target_pairs={{0,2},{1,3},{2,4},{3,5},{4,6},{5,7},{6,0},{7,1},{8,10},{9,11},{10,... | collective-permute-start | bytes 393224 | tf_op jit(solution)/shard_map/ppermute | solution.py:416
  118.2 9.8 %collective-permute-start.7 = (bf16[256,256]{1,0:T(8,128)(2,1)S(1)}, bf16[256,256]{1,0:T(8,128)(2,1)S(1)}, u32[]{:S(2)}, u32[]{:S(2)}) collective-permute-start(bf16[256,256]{1,0:T(8,128)(2,1)S(1)} %collective-permute-done.2.refs_1_), channel_id=1, source_target_pairs={{0,1},{1,2},{2,3},{3,4},{4,5},{5,6},{6,7},{7,0},{8,9},{9,10},{10,1... | collective-permute-start | bytes 393224 | tf_op jit(solution)/shard_map/ppermute | solution.py:416
  122.8 8.1 %collective-permute-start.8 = (bf16[256,256]{1,0:T(8,128)(2,1)S(1)}, bf16[256,256]{1,0:T(8,128)(2,1)S(1)}, u32[]{:S(2)}, u32[]{:S(2)}) collective-permute-start(bf16[256,256]{1,0:T(8,128)(2,1)S(1)} %collective-permute-done.3.refs_2_), channel_id=1, source_target_pairs={{0,7},{1,0},{2,1},{3,2},{4,3},{5,4},{6,5},{7,6},{8,15},{9,8},{10,9... | collective-permute-start | bytes 393224 | tf_op jit(solution)/shard_map/ppermute | solution.py:416

commit v6 on v5

--- a/solution.py
+++ b/solution.py
@@ -292,12 +292,20 @@
     out_ref[...] = current.astype(BF16).reshape(rows, chan, block)
 
 
-def turn_kernel(first_ref, second_ref, out_ref):
-    rows = out_ref.shape[0]
+def turn_kernel(first_ref, second_ref, out_ref, first, second, first_out, second_out, arrivals, departures):
     chan = out_ref.shape[1] // 2
-    for k, ref in enumerate((first_ref, second_ref)):
-        turned = jnp.transpose(ref[...].astype(F32)).astype(BF16)
-        out_ref[:, k * chan : (k + 1) * chan, :] = turned.reshape(rows, chan, -1)
+    moves = []
+    for k, (ref, held, turned) in enumerate(((first_ref, first, first_out), (second_ref, second, second_out))):
+        fetch = pltpu.make_async_copy(ref, held, arrivals.at[k])
+        fetch.start()
+        leave = pltpu.make_async_copy(turned, out_ref.at[:, pl.ds(k * chan, chan), :], departures.at[k])
+        moves.append((fetch, held, turned, leave))
+    for fetch, held, turned, leave in moves:
+        fetch.wait()
+        turned[...] = jnp.transpose(held[...].astype(F32)).astype(BF16).reshape(turned.shape)
+        leave.start()
+    for _, _, _, leave in moves:
+        leave.wait()
 
 
 def gate_kernel(mixed_ref, gate_ref, halo_ref, taps_ref, out_ref):
@@ -312,8 +320,10 @@
     out_ref[...] = (jnp.transpose(mixed_ref[...].astype(F32)) * factor).astype(BF16)
 
 
-def call(kernel, out_shape, scratch=(), flops=0, grant=None, placed=None):
+def call(kernel, out_shape, scratch=(), flops=0, grant=None, placed=None, result=None):
     specs = {} if placed is None else {"in_specs": [pl.BlockSpec(memory_space=space) for space in placed]}
+    if result is not None:
+        specs["out_specs"] = pl.BlockSpec(memory_space=result)
     return pl.pallas_call(
         kernel,
         out_shape=out_shape,
@@ -337,7 +347,16 @@
     bands = (features - 1) // 2
     into, back, pair, twiddle = tables(rows, chan, block)
 
-    turned = call(turn_kernel, jax.ShapeDtypeStruct((rows, 2 * chan, block), BF16))(values, gate_one)
+    vmem, anywhere = pltpu.VMEM, pl.ANY
+    turned = call(
+        turn_kernel,
+        jax.ShapeDtypeStruct((rows, 2 * chan, block), BF16),
+        [pltpu.VMEM((block, columns), BF16)] * 2
+        + [pltpu.VMEM((rows, chan, block), BF16)] * 2
+        + [pltpu.SemaphoreType.DMA((2,))] * 2,
+        placed=[anywhere] * 2,
+        result=anywhere,
+    )(values, gate_one)
     arrived = lax.all_to_all(turned, "row", 0, 0, tiled=True)
 
     down = [(k, k + 1) for k in range(rows - 1)]
@@ -357,7 +376,6 @@
     edge = (rows + 1) * chan
     parts = 2 * orders * chan
     spec_shape = jax.ShapeDtypeStruct((orders, edge, block), F32)
-    vmem, anywhere = pltpu.VMEM, pl.ANY
     spec_re, spec_im, param = call(
         functools.partial(filter_kernel, rows, chan),
         (spec_shape, spec_shape, jax.ShapeDtypeStruct((conv_taps.shape[0] + 1, chan, 4), F32)),
@@ -394,18 +412,22 @@
     return finish(gated, out_weight)
 
 
-def product_kernel(shifts, weight_ref, *refs):
+def product_kernel(shifts, weight_ref, before_ref, *refs):
     out_ref = refs[-1]
     peers = weight_ref.shape[0]
     me = lax.axis_index("col")
     half = out_ref.shape[0] // 2
     for part in range(2):
         place = slice(part * half, (part + 1) * half)
-        total = None
+        total = None if before_ref is None else before_ref[place, :]
         for shift, ref in zip(shifts, refs):
             term = dot(ref[place, :], weight_ref[lax.rem(me + (peers - shift), peers)])
             total = term if total is None else total + term
-        out_ref[place, :] = total.astype(BF16)
+        out_ref[place, :] = total.astype(out_ref.dtype)
+
+
+def first_product(shifts, weight_ref, *refs):
+    product_kernel(shifts, weight_ref, None, *refs)
 
 
 def finish(gated, out_weight):
@@ -422,12 +444,18 @@
     blocks[3] = shifted(blocks[2], 1)
     blocks[peers - 3] = shifted(blocks[peers - 2], peers - 1)
     weight = out_weight.reshape(peers, columns, -1)
+    near = (0, 2, peers - 2, 1, peers - 1)
+    far = (4, 3, peers - 3)
+    shape = (gated.shape[0], weight.shape[2])
+    total = call(
+        functools.partial(first_product, near),
+        jax.ShapeDtypeStruct(shape, F32),
+        flops=2_000_000_000,
+        grant=12 << 20,
+    )(weight, *(blocks[shift] for shift in near))
     return call(
-        functools.partial(product_kernel, tuple(blocks)),
-        jax.ShapeDtypeStruct((gated.shape[0], weight.shape[2]), BF16),
-        flops=1_000_000_000,
-        grant=12 << 20,
-    )(weight, *blocks.values())
+        functools.partial(product_kernel, far), jax.ShapeDtypeStruct(shape, BF16), flops=1_000_000_000, grant=12 << 20
+    )(weight, total, *(blocks[shift] for shift in far))
 
 
 def solution(mesh):

time: 133 us -> 133 us (level)
    pallas_call x2 -> x3, Pallas kernels: 3.23 us -> 3.41 us  [the longest x1 1.8 us: per_device(): call(turn_kernel, jax.ShapeDtypeStruct((rows, 2 * chan, block), BF16), [p...]
where the time goes in v6:
time: 133 us; the launch traced here: 132 us
  starting transfers between devices  80.9 us (61%)
  Pallas kernels  25.3 us (19%)
  waiting for transfers between devices  22.3 us (17%)
  local copies, waits for them, and re-layouts  3.37 us (3%)
    all_to_all x1, starting transfers between devices, per_device(): arrived = lax.all_to_all(turned, 'row', 0, 0, tiled=True)  44.5 us
    ppermute x7, starting transfers between devices, shifted(): lax.ppermute(block, 'col', [(k, (k + shift) % peers) for k in range(peers)])  25.4 us
    pallas_call x1, Pallas kernels, per_device(): call(functools.partial(filter_kernel, rows, chan), (spec_shape, spec_shap...  15.5 us
    all_to_all x1, waiting for transfers between devices, per_device(): lax.all_to_all(mixed, 'row', 0, 0, tiled=True).reshape(columns, block)  10.5 us
    all_to_all x1, starting transfers between devices, per_device(): lax.all_to_all(mixed, 'row', 0, 0, tiled=True).reshape(columns, block)  7.94 us
    pallas_call x1, Pallas kernels, per_device(): call(functools.partial(conv_kernel, rows, chan, orders), jax.ShapeDtypeSt...  6.24 us
    ppermute x7, waiting for transfers between devices, shifted(): lax.ppermute(block, 'col', [(k, (k + shift) % peers) for k in range(peers)])  5.04 us
    all_to_all x1, waiting for transfers between devices, per_device(): arrived = lax.all_to_all(turned, 'row', 0, 0, tiled=True)  4.5 us
  transfers between devices with their start and end apart: 11, of which 6 were waited for; matrix products, arithmetic and copies ran while one was open for 2% of the time, Pallas kernels for 12%

profile of v6, /device:TPU:80, one launch (start us, length us, event | category | flops | bytes accessed | tf_op | source)
XLA Modules:
  0.0 132.0 jit_solution(4919623485457764138)
XLA Ops:
  0.0 1.8 %shard_map.172 = bf16[32,16,256]{2,1,0:T(8,128)(2,1)} custom-call(bf16[256,256]{1,0:T(8,128)(2,1)} %first_ref.1, bf16[256,256]{1,0:T(8,128)(2,1)} %second_ref.1), custom_call_target="tpu_custom_call" | custom-call | tf_op jit(solution)/shard_map/pallas_call | solution.py:351
  1.8 44.5 %all-to-all-start = ((bf16[32,16,256]{2,1,0:T(8,128)(2,1)}), bf16[32,16,256]{2,1,0:T(8,128)(2,1)S(1)}, u32[]{:S(2)}, u32[]{:S(2)}) async-start(bf16[32,16,256]{2,1,0:T(8,128)(2,1)} %shard_map.172), calls=%async_computation | async-start | bytes 524288 | tf_op jit(solution)/shard_map/all_to_all | solution.py:360
  46.3 2.0 %copy.21 = f32[128,2,2,256]{3,0,2,1:T(8,128)} copy(f32[128,2,2,256]{3,2,1,0:T(2,128)} %param.27) | data formatting | bytes 1048576 | tf_op args[9]
  48.2 15.5 %shard_map.173 = (f32[2,264,256]{2,1,0:T(8,128)}, f32[2,264,256]{2,1,0:T(8,128)}, f32[4,8,4]{2,1,0:T(8,128)}) custom-call(f32[33,128]{1,0:T(8,128)} %embed_ref.1, f32[1,128]{1,0:T(1,128)} %bitcast.14, f32[1,128]{1,0:T(1,128)} %bitcast.15, f32[128,128]{1,0:T(8,128)} %inner_ref.1, f32[1,128]{1,0:T(1,128)} %bitcast.16, f32[2,2,128,256]{3,2,1,0:T(8,128)} %bitcast.13, ...), custom_call_target="tpu_custom_call" | custom-call | flops 12000000000 | tf_op jit(solution)/shard_map/pallas_call | solution.py:379
  63.8 4.5 %all-to-all-done.arrived_ref = bf16[32,16,256]{2,1,0:T(8,128)(2,1)S(1)} async-done(((bf16[32,16,256]{2,1,0:T(8,128)(2,1)}), bf16[32,16,256]{2,1,0:T(8,128)(2,1)S(1)}, u32[]{:S(2)}, u32[]{:S(2)}) %all-to-all-start) | async-done | bytes 262176 | tf_op jit(solution)/shard_map/all_to_all | solution.py:360
  68.3 0.7 copy-done.2
  69.0 6.2 %shard_map.174 = bf16[32,8,256]{2,1,0:T(8,128)(2,1)} custom-call(bf16[32,16,256]{2,1,0:T(8,128)(2,1)} %copy-done.2, f32[4,8,4]{2,1,0:T(8,128)} %get-tuple-element.8.param_ref, f32[2,264,256]{2,1,0:T(8,128)} %get-tuple-element.9.spec_re_ref, f32[2,264,256]{2,1,0:T(8,128)} %get-tuple-element.10.spec_im_ref, bf16[2,512,256]{2,1,0:T(8,128)(2,1)} %constant.11.clone.into_ref, ...), custom_call_target="tpu_custom_call" | custom-call | flops 5000000000 | tf_op jit(solution)/shard_map/pallas_call | solution.py:403
  75.2 7.9 %all-to-all-start.1 = ((bf16[32,8,256]{2,1,0:T(8,128)(2,1)}), bf16[32,8,256]{2,1,0:T(8,128)(2,1)S(1)}, u32[]{:S(2)}, u32[]{:S(2)}) async-start(bf16[32,8,256]{2,1,0:T(8,128)(2,1)} %shard_map.174), calls=%async_computation.1 | async-start | bytes 262144 | tf_op jit(solution)/shard_map/all_to_all | solution.py:408
  83.2 1.7 %collective-permute-start = (bf16[1,256]{1,0:T(2,128)(2,1)S(1)}, bf16[1,256]{1,0:T(2,128)(2,1)S(1)}, u32[]{:S(2)}, u32[]{:S(2)}) collective-permute-start(bf16[1,256]{1,0:T(2,128)(2,1)S(1)} %get-tuple-element.11), channel_id=1, source_target_pairs={{0,8},{8,16},{16,24},{24,32},{32,40},{40,48},{48,56},{56,64},{64,7... | collective-permute-start | bytes 1544 | tf_op jit(solution)/shard_map/ppermute | solution.py:364
  84.9 1.3 collective-permute-start.1
  86.3 0.7 slice_bitcast_fusion.taps_ref
  87.0 2.2 %collective-permute-done.1 = bf16[1,256]{1,0:T(2,128)(2,1)S(1)} collective-permute-done((bf16[1,256]{1,0:T(2,128)(2,1)S(1)}, bf16[1,256]{1,0:T(2,128)(2,1)S(1)}, u32[]{:S(2)}, u32[]{:S(2)}) %collective-permute-start.1) | collective-permute-done | bytes 544 | tf_op jit(solution)/shard_map/ppermute | solution.py:364
  89.2 10.5 %all-to-all-done.1 = bf16[32,8,256]{2,1,0:T(8,128)(2,1)S(1)} async-done(((bf16[32,8,256]{2,1,0:T(8,128)(2,1)}), bf16[32,8,256]{2,1,0:T(8,128)(2,1)S(1)}, u32[]{:S(2)}, u32[]{:S(2)}) %all-to-all-start.1) | async-done | bytes 131104 | tf_op jit(solution)/shard_map/all_to_all | solution.py:408
  99.8 4.6 %collective-permute-start.2 = (bf16[256,256]{1,0:T(8,128)(2,1)S(1)}, bf16[256,256]{1,0:T(8,128)(2,1)S(1)}, u32[]{:S(2)}, u32[]{:S(2)}) collective-permute-start(bf16[256,256]{1,0:T(8,128)(2,1)S(1)} %shard_map.175.refs_0_), channel_id=1, source_target_pairs={{0,2},{1,3},{2,4},{3,5},{4,6},{5,7},{6,0},{7,1},{8,10},{9,11},{10,... | collective-permute-start | bytes 393224 | tf_op jit(solution)/shard_map/ppermute | solution.py:438
  104.5 3.8 %collective-permute-start.3 = (bf16[256,256]{1,0:T(8,128)(2,1)S(1)}, bf16[256,256]{1,0:T(8,128)(2,1)S(1)}, u32[]{:S(2)}, u32[]{:S(2)}) collective-permute-start(bf16[256,256]{1,0:T(8,128)(2,1)S(1)} %shard_map.175.refs_0_), channel_id=1, source_target_pairs={{0,6},{1,7},{2,0},{3,1},{4,2},{5,3},{6,4},{7,5},{8,14},{9,15},{10,... | collective-permute-start | bytes 393224 | tf_op jit(solution)/shard_map/ppermute | solution.py:438
  108.3 3.1 %collective-permute-start.4 = (bf16[256,256]{1,0:T(8,128)(2,1)S(1)}, bf16[256,256]{1,0:T(8,128)(2,1)S(1)}, u32[]{:S(2)}, u32[]{:S(2)}) collective-permute-start(bf16[256,256]{1,0:T(8,128)(2,1)S(1)} %shard_map.175.refs_0_), channel_id=1, source_target_pairs={{0,1},{1,2},{2,3},{3,4},{4,5},{5,6},{6,7},{7,0},{8,9},{9,10},{10,1... | collective-permute-start | bytes 393224 | tf_op jit(solution)/shard_map/ppermute | solution.py:438
  111.4 4.0 %collective-permute-start.5 = (bf16[256,256]{1,0:T(8,128)(2,1)S(1)}, bf16[256,256]{1,0:T(8,128)(2,1)S(1)}, u32[]{:S(2)}, u32[]{:S(2)}) collective-permute-start(bf16[256,256]{1,0:T(8,128)(2,1)S(1)} %shard_map.175.refs_0_), channel_id=1, source_target_pairs={{0,7},{1,0},{2,1},{3,2},{4,3},{5,4},{6,5},{7,6},{8,15},{9,8},{10,9... | collective-permute-start | bytes 393224 | tf_op jit(solution)/shard_map/ppermute | solution.py:438
  115.4 2.8 %collective-permute-start.6 = (bf16[256,256]{1,0:T(8,128)(2,1)S(1)}, bf16[256,256]{1,0:T(8,128)(2,1)S(1)}, u32[]{:S(2)}, u32[]{:S(2)}) collective-permute-start(bf16[256,256]{1,0:T(8,128)(2,1)S(1)} %collective-permute-done.2.refs_1_), channel_id=1, source_target_pairs={{0,2},{1,3},{2,4},{3,5},{4,6},{5,7},{6,0},{7,1},{8,10},{9,11},{10,... | collective-permute-start | bytes 393224 | tf_op jit(solution)/shard_map/ppermute | solution.py:438
  118.2 4.6 %collective-permute-start.7 = (bf16[256,256]{1,0:T(8,128)(2,1)S(1)}, bf16[256,256]{1,0:T(8,128)(2,1)S(1)}, u32[]{:S(2)}, u32[]{:S(2)}) collective-permute-start(bf16[256,256]{1,0:T(8,128)(2,1)S(1)} %collective-permute-done.2.refs_1_), channel_id=1, source_target_pairs={{0,1},{1,2},{2,3},{3,4},{4,5},{5,6},{6,7},{7,0},{8,9},{9,10},{10,1... | collective-permute-start | bytes 393224 | tf_op jit(solution)/shard_map/ppermute | solution.py:438
  122.8 2.5 %collective-permute-start.8 = (bf16[256,256]{1,0:T(8,128)(2,1)S(1)}, bf16[256,256]{1,0:T(8,128)(2,1)S(1)}, u32[]{:S(2)}, u32[]{:S(2)}) collective-permute-start(bf16[256,256]{1,0:T(8,128)(2,1)S(1)} %collective-permute-done.3.refs_2_), channel_id=1, source_target_pairs={{0,7},{1,0},{2,1},{3,2},{4,3},{5,4},{6,5},{7,6},{8,15},{9,8},{10,9... | collective-permute-start | bytes 393224 | tf_op jit(solution)/shard_map/ppermute | solution.py:438
  125.9 0.7 collective-permute-done.6.refs_0_
  126.6 1.4 %collective-permute-done.7.refs_1_ = bf16[256,256]{1,0:T(8,128)(2,1)S(1)} collective-permute-done((bf16[256,256]{1,0:T(8,128)(2,1)S(1)}, bf16[256,256]{1,0:T(8,128)(2,1)S(1)}, u32[]{:S(2)}, u32[]{:S(2)}) %collective-permute-start.7) | collective-permute-done | bytes 131104 | tf_op jit(solution)/shard_map/ppermute | solution.py:438
  128.0 2.9 %collective-permute-done.8.refs_2_ = bf16[256,256]{1,0:T(8,128)(2,1)S(1)} collective-permute-done((bf16[256,256]{1,0:T(8,128)(2,1)S(1)}, bf16[256,256]{1,0:T(8,128)(2,1)S(1)}, u32[]{:S(2)}, u32[]{:S(2)}) %collective-permute-start.8) | collective-permute-done | bytes 131104 | tf_op jit(solution)/shard_map/ppermute | solution.py:438
  130.9 1.1 shard_map.177
  (14 shorter events, 0.7 us)
Async XLA Ops:
  1.8 66.5 %all-to-all-start = ((bf16[32,16,256]{2,1,0:T(8,128)(2,1)}), bf16[32,16,256]{2,1,0:T(8,128)(2,1)S(1)}, u32[]{:S(2)}, u32[]{:S(2)}) async-start(bf16[32,16,256]{2,1,0:T(8,128)(2,1)} %shard_map.172), calls=%async_computation | async-start | bytes 524288 | tf_op jit(solution)/shard_map/all_to_all | solution.py:360
  68.3 0.7 copy-start.2
  69.0 14.2 %copy-start = (bf16[256,256]{1,0:T(8,128)(2,1)S(1)}, bf16[256,256]{1,0:T(8,128)(2,1)}, u32[]{:S(2)}) copy-start(bf16[256,256]{1,0:T(8,128)(2,1)} %gate_ref.1) | copy-start | bytes 393220
  69.0 56.4 %copy-start.1 = (bf16[2048,512]{1,0:T(8,128)(2,1)S(1)}, bf16[2048,512]{1,0:T(8,128)(2,1)}, u32[]{:S(2)}) copy-start(bf16[2048,512]{1,0:T(8,128)(2,1)} %param.30) | copy-start | bytes 6291460
  75.2 24.5 %all-to-all-start.1 = ((bf16[32,8,256]{2,1,0:T(8,128)(2,1)}), bf16[32,8,256]{2,1,0:T(8,128)(2,1)S(1)}, u32[]{:S(2)}, u32[]{:S(2)}) async-start(bf16[32,8,256]{2,1,0:T(8,128)(2,1)} %shard_map.174), calls=%async_computation.1 | async-start | bytes 262144 | tf_op jit(solution)/shard_map/all_to_all | solution.py:408
  83.2 3.8 %collective-permute-start = (bf16[1,256]{1,0:T(2,128)(2,1)S(1)}, bf16[1,256]{1,0:T(2,128)(2,1)S(1)}, u32[]{:S(2)}, u32[]{:S(2)}) collective-permute-start(bf16[1,256]{1,0:T(2,128)(2,1)S(1)} %get-tuple-element.11), channel_id=1, source_target_pairs={{0,8},{8,16},{16,24},{24,32},{32,40},{40,48},{48,56},{56,64},{64,7... | collective-permute-start | bytes 1544 | tf_op jit(solution)/shard_map/ppermute | solution.py:364
  84.9 4.2 %collective-permute-start.1 = (bf16[1,256]{1,0:T(2,128)(2,1)S(1)}, bf16[1,256]{1,0:T(2,128)(2,1)S(1)}, u32[]{:S(2)}, u32[]{:S(2)}) collective-permute-start(bf16[1,256]{1,0:T(2,128)(2,1)S(1)} %get-tuple-element.12), channel_id=1, source_target_pairs={{8,0},{16,8},{24,16},{32,24},{40,32},{48,40},{56,48},{64,56},{72,6... | collective-permute-start | bytes 1544 | tf_op jit(solution)/shard_map/ppermute | solution.py:364
  99.8 15.6 %collective-permute-start.2 = (bf16[256,256]{1,0:T(8,128)(2,1)S(1)}, bf16[256,256]{1,0:T(8,128)(2,1)S(1)}, u32[]{:S(2)}, u32[]{:S(2)}) collective-permute-start(bf16[256,256]{1,0:T(8,128)(2,1)S(1)} %shard_map.175.refs_0_), channel_id=1, source_target_pairs={{0,2},{1,3},{2,4},{3,5},{4,6},{5,7},{6,0},{7,1},{8,10},{9,11},{10,... | collective-permute-start | bytes 393224 | tf_op jit(solution)/shard_map/ppermute | solution.py:438
  104.5 18.4 %collective-permute-start.3 = (bf16[256,256]{1,0:T(8,128)(2,1)S(1)}, bf16[256,256]{1,0:T(8,128)(2,1)S(1)}, u32[]{:S(2)}, u32[]{:S(2)}) collective-permute-start(bf16[256,256]{1,0:T(8,128)(2,1)S(1)} %shard_map.175.refs_0_), channel_id=1, source_target_pairs={{0,6},{1,7},{2,0},{3,1},{4,2},{5,3},{6,4},{7,5},{8,14},{9,15},{10,... | collective-permute-start | bytes 393224 | tf_op jit(solution)/shard_map/ppermute | solution.py:438
  108.3 17.1 %collective-permute-start.4 = (bf16[256,256]{1,0:T(8,128)(2,1)S(1)}, bf16[256,256]{1,0:T(8,128)(2,1)S(1)}, u32[]{:S(2)}, u32[]{:S(2)}) collective-permute-start(bf16[256,256]{1,0:T(8,128)(2,1)S(1)} %shard_map.175.refs_0_), channel_id=1, source_target_pairs={{0,1},{1,2},{2,3},{3,4},{4,5},{5,6},{6,7},{7,0},{8,9},{9,10},{10,1... | collective-permute-start | bytes 393224 | tf_op jit(solution)/shard_map/ppermute | solution.py:438
  111.4 13.9 %collective-permute-start.5 = (bf16[256,256]{1,0:T(8,128)(2,1)S(1)}, bf16[256,256]{1,0:T(8,128)(2,1)S(1)}, u32[]{:S(2)}, u32[]{:S(2)}) collective-permute-start(bf16[256,256]{1,0:T(8,128)(2,1)S(1)} %shard_map.175.refs_0_), channel_id=1, source_target_pairs={{0,7},{1,0},{2,1},{3,2},{4,3},{5,4},{6,5},{7,6},{8,15},{9,8},{10,9... | collective-permute-start | bytes 393224 | tf_op jit(solution)/shard_map/ppermute | solution.py:438
  115.4 11.2 %collective-permute-start.6 = (bf16[256,256]{1,0:T(8,128)(2,1)S(1)}, bf16[256,256]{1,0:T(8,128)(2,1)S(1)}, u32[]{:S(2)}, u32[]{:S(2)}) collective-permute-start(bf16[256,256]{1,0:T(8,128)(2,1)S(1)} %collective-permute-done.2.refs_1_), channel_id=1, source_target_pairs={{0,2},{1,3},{2,4},{3,5},{4,6},{5,7},{6,0},{7,1},{8,10},{9,11},{10,... | collective-permute-start | bytes 393224 | tf_op jit(solution)/shard_map/ppermute | solution.py:438
  118.2 9.8 %collective-permute-start.7 = (bf16[256,256]{1,0:T(8,128)(2,1)S(1)}, bf16[256,256]{1,0:T(8,128)(2,1)S(1)}, u32[]{:S(2)}, u32[]{:S(2)}) collective-permute-start(bf16[256,256]{1,0:T(8,128)(2,1)S(1)} %collective-permute-done.2.refs_1_), channel_id=1, source_target_pairs={{0,1},{1,2},{2,3},{3,4},{4,5},{5,6},{6,7},{7,0},{8,9},{9,10},{10,1... | collective-permute-start | bytes 393224 | tf_op jit(solution)/shard_map/ppermute | solution.py:438
  122.8 8.1 %collective-permute-start.8 = (bf16[256,256]{1,0:T(8,128)(2,1)S(1)}, bf16[256,256]{1,0:T(8,128)(2,1)S(1)}, u32[]{:S(2)}, u32[]{:S(2)}) collective-permute-start(bf16[256,256]{1,0:T(8,128)(2,1)S(1)} %collective-permute-done.3.refs_2_), channel_id=1, source_target_pairs={{0,7},{1,0},{2,1},{3,2},{4,3},{5,4},{6,5},{7,6},{8,15},{9,8},{10,9... | collective-permute-start | bytes 393224 | tf_op jit(solution)/shard_map/ppermute | solution.py:438

commit v7 on v6

--- a/solution.py
+++ b/solution.py
@@ -404,6 +404,7 @@
         functools.partial(conv_kernel, rows, chan, orders),
         jax.ShapeDtypeStruct((rows, chan, block), BF16),
         flops=5_000_000_000,
+        grant=53 << 20,
     )(arrived, param, spec_re, spec_im, into, back, pair, twiddle)
     mixed = lax.all_to_all(mixed, "row", 0, 0, tiled=True).reshape(columns, block)
     gated = call(gate_kernel, jax.ShapeDtypeStruct((block, columns), BF16), grant=12 << 20)(

time: 133 us -> 133 us (level)
    unnamed x7 -> x9, local copies, waits for them, and re-layouts: 2.67 us -> 2.69 us
where the time goes in v7:
time: 133 us; the launch traced here: 132 us
  starting transfers between devices  80.9 us (61%)
  Pallas kernels  25.2 us (19%)
  waiting for transfers between devices  22.3 us (17%)
  local copies, waits for them, and re-layouts  3.38 us (3%)
    all_to_all x1, starting transfers between devices, per_device(): arrived = lax.all_to_all(turned, 'row', 0, 0, tiled=True)  44.5 us
    ppermute x7, starting transfers between devices, shifted(): lax.ppermute(block, 'col', [(k, (k + shift) % peers) for k in range(peers)])  25.4 us
    pallas_call x1, Pallas kernels, per_device(): call(functools.partial(filter_kernel, rows, chan), (spec_shape, spec_shap...  15.5 us
    all_to_all x1, waiting for transfers between devices, per_device(): lax.all_to_all(mixed, 'row', 0, 0, tiled=True).reshape(columns, block)  10.5 us
    all_to_all x1, starting transfers between devices, per_device(): lax.all_to_all(mixed, 'row', 0, 0, tiled=True).reshape(columns, block)  7.95 us
    pallas_call x1, Pallas kernels, per_device(): call(functools.partial(conv_kernel, rows, chan, orders), jax.ShapeDtypeSt...  6.15 us
    ppermute x7, waiting for transfers between devices, shifted(): lax.ppermute(block, 'col', [(k, (k + shift) % peers) for k in range(peers)])  5.05 us
    all_to_all x1, waiting for transfers between devices, per_device(): arrived = lax.all_to_all(turned, 'row', 0, 0, tiled=True)  4.49 us
  transfers between devices with their start and end apart: 11, of which 6 were waited for; matrix products, arithmetic and copies ran while one was open for 2% of the time, Pallas kernels for 12%

profile of v7, /device:TPU:80, one launch (start us, length us, event | category | flops | bytes accessed | tf_op | source)
XLA Modules:
  0.0 131.9 jit_solution(11267401385074545186)
XLA Ops:
  0.0 1.8 %shard_map.172 = bf16[32,16,256]{2,1,0:T(8,128)(2,1)} custom-call(bf16[256,256]{1,0:T(8,128)(2,1)} %first_ref.1, bf16[256,256]{1,0:T(8,128)(2,1)} %second_ref.1), custom_call_target="tpu_custom_call" | custom-call | tf_op jit(solution)/shard_map/pallas_call | solution.py:351
  1.8 44.5 %all-to-all-start = ((bf16[32,16,256]{2,1,0:T(8,128)(2,1)}), bf16[32,16,256]{2,1,0:T(8,128)(2,1)S(1)}, u32[]{:S(2)}, u32[]{:S(2)}) async-start(bf16[32,16,256]{2,1,0:T(8,128)(2,1)} %shard_map.172), calls=%async_computation | async-start | bytes 524288 | tf_op jit(solution)/shard_map/all_to_all | solution.py:360
  46.3 2.0 %copy.21 = f32[128,2,2,256]{3,0,2,1:T(8,128)} copy(f32[128,2,2,256]{3,2,1,0:T(2,128)} %param.27) | data formatting | bytes 1048576 | tf_op args[9]
  48.2 15.5 %shard_map.173 = (f32[2,264,256]{2,1,0:T(8,128)}, f32[2,264,256]{2,1,0:T(8,128)}, f32[4,8,4]{2,1,0:T(8,128)}) custom-call(f32[33,128]{1,0:T(8,128)} %embed_ref.1, f32[1,128]{1,0:T(1,128)} %bitcast.14, f32[1,128]{1,0:T(1,128)} %bitcast.15, f32[128,128]{1,0:T(8,128)} %inner_ref.1, f32[1,128]{1,0:T(1,128)} %bitcast.16, f32[2,2,128,256]{3,2,1,0:T(8,128)} %bitcast.13, ...), custom_call_target="tpu_custom_call" | custom-call | flops 12000000000 | tf_op jit(solution)/shard_map/pallas_call | solution.py:379
  63.8 4.5 %all-to-all-done.arrived_ref = bf16[32,16,256]{2,1,0:T(8,128)(2,1)S(1)} async-done(((bf16[32,16,256]{2,1,0:T(8,128)(2,1)}), bf16[32,16,256]{2,1,0:T(8,128)(2,1)S(1)}, u32[]{:S(2)}, u32[]{:S(2)}) %all-to-all-start) | async-done | bytes 262176 | tf_op jit(solution)/shard_map/all_to_all | solution.py:360
  68.3 0.7 copy-done.3
  69.0 6.1 %shard_map.174 = bf16[32,8,256]{2,1,0:T(8,128)(2,1)} custom-call(bf16[32,16,256]{2,1,0:T(8,128)(2,1)S(1)} %all-to-all-done.arrived_ref, f32[4,8,4]{2,1,0:T(8,128)S(1)} %copy-done.3, f32[2,264,256]{2,1,0:T(8,128)} %get-tuple-element.9.spec_re_ref, f32[2,264,256]{2,1,0:T(8,128)} %get-tuple-element.10.spec_im_ref, ...), custom_call_target="tpu_custom_call" | custom-call | flops 5000000000 | tf_op jit(solution)/shard_map/pallas_call | solution.py:403
  75.1 7.9 %all-to-all-start.1 = ((bf16[32,8,256]{2,1,0:T(8,128)(2,1)}), bf16[32,8,256]{2,1,0:T(8,128)(2,1)S(1)}, u32[]{:S(2)}, u32[]{:S(2)}) async-start(bf16[32,8,256]{2,1,0:T(8,128)(2,1)} %shard_map.174), calls=%async_computation.1 | async-start | bytes 262144 | tf_op jit(solution)/shard_map/all_to_all | solution.py:409
  83.1 1.7 %collective-permute-start = (bf16[1,256]{1,0:T(2,128)(2,1)S(1)}, bf16[1,256]{1,0:T(2,128)(2,1)S(1)}, u32[]{:S(2)}, u32[]{:S(2)}) collective-permute-start(bf16[1,256]{1,0:T(2,128)(2,1)S(1)} %get-tuple-element.11), channel_id=1, source_target_pairs={{0,8},{8,16},{16,24},{24,32},{32,40},{40,48},{48,56},{56,64},{64,7... | collective-permute-start | bytes 1544 | tf_op jit(solution)/shard_map/ppermute | solution.py:364
  84.9 1.3 collective-permute-start.1
  86.2 0.7 slice_bitcast_fusion.taps_ref
  86.9 2.2 %collective-permute-done.1 = bf16[1,256]{1,0:T(2,128)(2,1)S(1)} collective-permute-done((bf16[1,256]{1,0:T(2,128)(2,1)S(1)}, bf16[1,256]{1,0:T(2,128)(2,1)S(1)}, u32[]{:S(2)}, u32[]{:S(2)}) %collective-permute-start.1) | collective-permute-done | bytes 544 | tf_op jit(solution)/shard_map/ppermute | solution.py:364
  89.1 10.5 %all-to-all-done.1 = bf16[32,8,256]{2,1,0:T(8,128)(2,1)S(1)} async-done(((bf16[32,8,256]{2,1,0:T(8,128)(2,1)}), bf16[32,8,256]{2,1,0:T(8,128)(2,1)S(1)}, u32[]{:S(2)}, u32[]{:S(2)}) %all-to-all-start.1) | async-done | bytes 131104 | tf_op jit(solution)/shard_map/all_to_all | solution.py:409
  99.8 4.6 %collective-permute-start.2 = (bf16[256,256]{1,0:T(8,128)(2,1)S(1)}, bf16[256,256]{1,0:T(8,128)(2,1)S(1)}, u32[]{:S(2)}, u32[]{:S(2)}) collective-permute-start(bf16[256,256]{1,0:T(8,128)(2,1)S(1)} %shard_map.175.refs_0_), channel_id=1, source_target_pairs={{0,2},{1,3},{2,4},{3,5},{4,6},{5,7},{6,0},{7,1},{8,10},{9,11},{10,... | collective-permute-start | bytes 393224 | tf_op jit(solution)/shard_map/ppermute | solution.py:439
  104.4 3.8 %collective-permute-start.3 = (bf16[256,256]{1,0:T(8,128)(2,1)S(1)}, bf16[256,256]{1,0:T(8,128)(2,1)S(1)}, u32[]{:S(2)}, u32[]{:S(2)}) collective-permute-start(bf16[256,256]{1,0:T(8,128)(2,1)S(1)} %shard_map.175.refs_0_), channel_id=1, source_target_pairs={{0,6},{1,7},{2,0},{3,1},{4,2},{5,3},{6,4},{7,5},{8,14},{9,15},{10,... | collective-permute-start | bytes 393224 | tf_op jit(solution)/shard_map/ppermute | solution.py:439
  108.2 3.1 %collective-permute-start.4 = (bf16[256,256]{1,0:T(8,128)(2,1)S(1)}, bf16[256,256]{1,0:T(8,128)(2,1)S(1)}, u32[]{:S(2)}, u32[]{:S(2)}) collective-permute-start(bf16[256,256]{1,0:T(8,128)(2,1)S(1)} %shard_map.175.refs_0_), channel_id=1, source_target_pairs={{0,1},{1,2},{2,3},{3,4},{4,5},{5,6},{6,7},{7,0},{8,9},{9,10},{10,1... | collective-permute-start | bytes 393224 | tf_op jit(solution)/shard_map/ppermute | solution.py:439
  111.4 4.0 %collective-permute-start.5 = (bf16[256,256]{1,0:T(8,128)(2,1)S(1)}, bf16[256,256]{1,0:T(8,128)(2,1)S(1)}, u32[]{:S(2)}, u32[]{:S(2)}) collective-permute-start(bf16[256,256]{1,0:T(8,128)(2,1)S(1)} %shard_map.175.refs_0_), channel_id=1, source_target_pairs={{0,7},{1,0},{2,1},{3,2},{4,3},{5,4},{6,5},{7,6},{8,15},{9,8},{10,9... | collective-permute-start | bytes 393224 | tf_op jit(solution)/shard_map/ppermute | solution.py:439
  115.4 2.8 %collective-permute-start.6 = (bf16[256,256]{1,0:T(8,128)(2,1)S(1)}, bf16[256,256]{1,0:T(8,128)(2,1)S(1)}, u32[]{:S(2)}, u32[]{:S(2)}) collective-permute-start(bf16[256,256]{1,0:T(8,128)(2,1)S(1)} %collective-permute-done.2.refs_1_), channel_id=1, source_target_pairs={{0,2},{1,3},{2,4},{3,5},{4,6},{5,7},{6,0},{7,1},{8,10},{9,11},{10,... | collective-permute-start | bytes 393224 | tf_op jit(solution)/shard_map/ppermute | solution.py:439
  118.1 4.6 %collective-permute-start.7 = (bf16[256,256]{1,0:T(8,128)(2,1)S(1)}, bf16[256,256]{1,0:T(8,128)(2,1)S(1)}, u32[]{:S(2)}, u32[]{:S(2)}) collective-permute-start(bf16[256,256]{1,0:T(8,128)(2,1)S(1)} %collective-permute-done.2.refs_1_), channel_id=1, source_target_pairs={{0,1},{1,2},{2,3},{3,4},{4,5},{5,6},{6,7},{7,0},{8,9},{9,10},{10,1... | collective-permute-start | bytes 393224 | tf_op jit(solution)/shard_map/ppermute | solution.py:439
  122.8 2.5 %collective-permute-start.8 = (bf16[256,256]{1,0:T(8,128)(2,1)S(1)}, bf16[256,256]{1,0:T(8,128)(2,1)S(1)}, u32[]{:S(2)}, u32[]{:S(2)}) collective-permute-start(bf16[256,256]{1,0:T(8,128)(2,1)S(1)} %collective-permute-done.3.refs_2_), channel_id=1, source_target_pairs={{0,7},{1,0},{2,1},{3,2},{4,3},{5,4},{6,5},{7,6},{8,15},{9,8},{10,9... | collective-permute-start | bytes 393224 | tf_op jit(solution)/shard_map/ppermute | solution.py:439
  125.8 0.7 collective-permute-done.6.refs_0_
  126.5 1.4 %collective-permute-done.7.refs_1_ = bf16[256,256]{1,0:T(8,128)(2,1)S(1)} collective-permute-done((bf16[256,256]{1,0:T(8,128)(2,1)S(1)}, bf16[256,256]{1,0:T(8,128)(2,1)S(1)}, u32[]{:S(2)}, u32[]{:S(2)}) %collective-permute-start.7) | collective-permute-done | bytes 131104 | tf_op jit(solution)/shard_map/ppermute | solution.py:439
  128.0 2.9 %collective-permute-done.8.refs_2_ = bf16[256,256]{1,0:T(8,128)(2,1)S(1)} collective-permute-done((bf16[256,256]{1,0:T(8,128)(2,1)S(1)}, bf16[256,256]{1,0:T(8,128)(2,1)S(1)}, u32[]{:S(2)}, u32[]{:S(2)}) %collective-permute-start.8) | collective-permute-done | bytes 131104 | tf_op jit(solution)/shard_map/ppermute | solution.py:439
  130.9 1.1 shard_map.177
  (16 shorter events, 0.7 us)
Async XLA Ops:
  1.8 66.5 %all-to-all-start = ((bf16[32,16,256]{2,1,0:T(8,128)(2,1)}), bf16[32,16,256]{2,1,0:T(8,128)(2,1)S(1)}, u32[]{:S(2)}, u32[]{:S(2)}) async-start(bf16[32,16,256]{2,1,0:T(8,128)(2,1)} %shard_map.172), calls=%async_computation | async-start | bytes 524288 | tf_op jit(solution)/shard_map/all_to_all | solution.py:360
  48.2 20.0 %copy-start.2 = (f32[2,33,256]{2,1,0:T(8,128)S(1)}, f32[2,33,256]{2,1,0:T(8,128)}, u32[]{:S(2)}) copy-start(f32[2,33,256]{2,1,0:T(8,128)} %constant.13.clone.twiddle_ref) | copy-start | bytes 202756
  68.3 0.7 copy-start.3
  69.0 14.1 %copy-start = (bf16[256,256]{1,0:T(8,128)(2,1)S(1)}, bf16[256,256]{1,0:T(8,128)(2,1)}, u32[]{:S(2)}) copy-start(bf16[256,256]{1,0:T(8,128)(2,1)} %gate_ref.1) | copy-start | bytes 393220
  69.0 56.3 %copy-start.1 = (bf16[2048,512]{1,0:T(8,128)(2,1)S(1)}, bf16[2048,512]{1,0:T(8,128)(2,1)}, u32[]{:S(2)}) copy-start(bf16[2048,512]{1,0:T(8,128)(2,1)} %param.30) | copy-start | bytes 6291460
  75.1 24.5 %all-to-all-start.1 = ((bf16[32,8,256]{2,1,0:T(8,128)(2,1)}), bf16[32,8,256]{2,1,0:T(8,128)(2,1)S(1)}, u32[]{:S(2)}, u32[]{:S(2)}) async-start(bf16[32,8,256]{2,1,0:T(8,128)(2,1)} %shard_map.174), calls=%async_computation.1 | async-start | bytes 262144 | tf_op jit(solution)/shard_map/all_to_all | solution.py:409
  83.1 3.8 %collective-permute-start = (bf16[1,256]{1,0:T(2,128)(2,1)S(1)}, bf16[1,256]{1,0:T(2,128)(2,1)S(1)}, u32[]{:S(2)}, u32[]{:S(2)}) collective-permute-start(bf16[1,256]{1,0:T(2,128)(2,1)S(1)} %get-tuple-element.11), channel_id=1, source_target_pairs={{0,8},{8,16},{16,24},{24,32},{32,40},{40,48},{48,56},{56,64},{64,7... | collective-permute-start | bytes 1544 | tf_op jit(solution)/shard_map/ppermute | solution.py:364
  84.9 4.2 %collective-permute-start.1 = (bf16[1,256]{1,0:T(2,128)(2,1)S(1)}, bf16[1,256]{1,0:T(2,128)(2,1)S(1)}, u32[]{:S(2)}, u32[]{:S(2)}) collective-permute-start(bf16[1,256]{1,0:T(2,128)(2,1)S(1)} %get-tuple-element.12), channel_id=1, source_target_pairs={{8,0},{16,8},{24,16},{32,24},{40,32},{48,40},{56,48},{64,56},{72,6... | collective-permute-start | bytes 1544 | tf_op jit(solution)/shard_map/ppermute | solution.py:364
  99.8 15.6 %collective-permute-start.2 = (bf16[256,256]{1,0:T(8,128)(2,1)S(1)}, bf16[256,256]{1,0:T(8,128)(2,1)S(1)}, u32[]{:S(2)}, u32[]{:S(2)}) collective-permute-start(bf16[256,256]{1,0:T(8,128)(2,1)S(1)} %shard_map.175.refs_0_), channel_id=1, source_target_pairs={{0,2},{1,3},{2,4},{3,5},{4,6},{5,7},{6,0},{7,1},{8,10},{9,11},{10,... | collective-permute-start | bytes 393224 | tf_op jit(solution)/shard_map/ppermute | solution.py:439
  104.4 18.4 %collective-permute-start.3 = (bf16[256,256]{1,0:T(8,128)(2,1)S(1)}, bf16[256,256]{1,0:T(8,128)(2,1)S(1)}, u32[]{:S(2)}, u32[]{:S(2)}) collective-permute-start(bf16[256,256]{1,0:T(8,128)(2,1)S(1)} %shard_map.175.refs_0_), channel_id=1, source_target_pairs={{0,6},{1,7},{2,0},{3,1},{4,2},{5,3},{6,4},{7,5},{8,14},{9,15},{10,... | collective-permute-start | bytes 393224 | tf_op jit(solution)/shard_map/ppermute | solution.py:439
  108.2 17.0 %collective-permute-start.4 = (bf16[256,256]{1,0:T(8,128)(2,1)S(1)}, bf16[256,256]{1,0:T(8,128)(2,1)S(1)}, u32[]{:S(2)}, u32[]{:S(2)}) collective-permute-start(bf16[256,256]{1,0:T(8,128)(2,1)S(1)} %shard_map.175.refs_0_), channel_id=1, source_target_pairs={{0,1},{1,2},{2,3},{3,4},{4,5},{5,6},{6,7},{7,0},{8,9},{9,10},{10,1... | collective-permute-start | bytes 393224 | tf_op jit(solution)/shard_map/ppermute | solution.py:439
  111.4 13.9 %collective-permute-start.5 = (bf16[256,256]{1,0:T(8,128)(2,1)S(1)}, bf16[256,256]{1,0:T(8,128)(2,1)S(1)}, u32[]{:S(2)}, u32[]{:S(2)}) collective-permute-start(bf16[256,256]{1,0:T(8,128)(2,1)S(1)} %shard_map.175.refs_0_), channel_id=1, source_target_pairs={{0,7},{1,0},{2,1},{3,2},{4,3},{5,4},{6,5},{7,6},{8,15},{9,8},{10,9... | collective-permute-start | bytes 393224 | tf_op jit(solution)/shard_map/ppermute | solution.py:439
  115.4 11.2 %collective-permute-start.6 = (bf16[256,256]{1,0:T(8,128)(2,1)S(1)}, bf16[256,256]{1,0:T(8,128)(2,1)S(1)}, u32[]{:S(2)}, u32[]{:S(2)}) collective-permute-start(bf16[256,256]{1,0:T(8,128)(2,1)S(1)} %collective-permute-done.2.refs_1_), channel_id=1, source_target_pairs={{0,2},{1,3},{2,4},{3,5},{4,6},{5,7},{6,0},{7,1},{8,10},{9,11},{10,... | collective-permute-start | bytes 393224 | tf_op jit(solution)/shard_map/ppermute | solution.py:439
  118.1 9.8 %collective-permute-start.7 = (bf16[256,256]{1,0:T(8,128)(2,1)S(1)}, bf16[256,256]{1,0:T(8,128)(2,1)S(1)}, u32[]{:S(2)}, u32[]{:S(2)}) collective-permute-start(bf16[256,256]{1,0:T(8,128)(2,1)S(1)} %collective-permute-done.2.refs_1_), channel_id=1, source_target_pairs={{0,1},{1,2},{2,3},{3,4},{4,5},{5,6},{6,7},{7,0},{8,9},{9,10},{10,1... | collective-permute-start | bytes 393224 | tf_op jit(solution)/shard_map/ppermute | solution.py:439
  122.8 8.1 %collective-permute-start.8 = (bf16[256,256]{1,0:T(8,128)(2,1)S(1)}, bf16[256,256]{1,0:T(8,128)(2,1)S(1)}, u32[]{:S(2)}, u32[]{:S(2)}) collective-permute-start(bf16[256,256]{1,0:T(8,128)(2,1)S(1)} %collective-permute-done.3.refs_2_), channel_id=1, source_target_pairs={{0,7},{1,0},{2,1},{3,2},{4,3},{5,4},{6,5},{7,6},{8,15},{9,8},{10,9... | collective-permute-start | bytes 393224 | tf_op jit(solution)/shard_map/ppermute | solution.py:439
